TPU v7x, 32 devices: a whole 2x2x4 slice. The times are simulated.
32 devices in a mesh: sp: 4 (over z), tp: 8 (over y, x, core).
Axes of the slice: x: 2, y: 2, z: 4, core: 2. Of those that a mesh axis runs over, the one named last changes fastest.
Arguments:
- target_rows: bfloat16 [768, 2048], P(('sp', 'tp')), may hold values from -6 to 6
- source_rows: bfloat16 [4096, 2048], P(('sp', 'tp')), may hold values from -6 to 6
- target_gain: float32 [2048], replicated, may hold values from 0.55 to 9
- source_gain: float32 [2048], replicated, may hold values from 0.55 to 9
- query_weight: bfloat16 [2048, 2048], P(None, 'tp'), may hold values from -0.125 to 0.125
- key_weight: bfloat16 [2048, 512], P('tp'), may hold values from -0.125 to 0.125
- value_weight: bfloat16 [2048, 512], P('tp'), may hold values from -0.125 to 0.125
- out_weight: bfloat16 [2048, 2048], P('tp'), may hold values from -0.125 to 0.125
- out_cotangent: bfloat16 [768, 2048], P(('sp', 'tp')), may hold values from -6 to 6
Outputs:
- target_grad: float32 [768, 2048], P(('sp', 'tp'))
- source_grad: float32 [4096, 2048], P(('sp', 'tp'))
- out_weight_grad: float32 [2048, 2048], P('tp')
All inputs are finite; a program needn't handle non-finite values.
Results may differ from a plain program's by a relative error of at most 0.03.
Values may be sent and summed in bfloat16 or wider, within the bound.
A program may use at most 64 MiB of HBM per device.

v0:
```python
import jax
import jax.numpy as jnp
from jax import lax
from jax.sharding import PartitionSpec as P

HEAD_DIM = 64
KV_HEADS = 8


EPSILON = 1e-06
NEGATIVE = -1e30


def normalize(matrix, gain_vector):
    widened = matrix.astype(jnp.float32)
    factor = lax.rsqrt(jnp.mean(widened * widened, axis=-1, keepdims=True) + EPSILON)
    return (widened * factor * gain_vector).astype(jnp.bfloat16)


def norm_back(matrix, gain_vector, upstream):
    widened = matrix.astype(jnp.float32)
    factor = lax.rsqrt(jnp.mean(widened * widened, axis=-1, keepdims=True) + EPSILON)
    weighted = upstream * gain_vector
    inner_sum = jnp.mean(weighted * widened, axis=-1, keepdims=True)
    return factor * weighted - widened * factor**3 * inner_sum


def block_rows_for(length):
    return 512 if length % 512 == 0 else length


def body(
    target_rows,
    source_rows,
    target_gain,
    source_gain,
    query_weight,
    key_weight,
    value_weight,
    out_weight,
    out_cotangent,
):
    tp_count = lax.axis_size("tp")
    local_heads = query_weight.shape[1] // HEAD_DIM
    slot_heads = max(1, KV_HEADS // tp_count)
    copies = max(1, tp_count // KV_HEADS)
    per_slot = local_heads // slot_heads
    score_scale = HEAD_DIM ** (-0.5)
    normed_t = normalize(target_rows, target_gain)
    normed_s = normalize(source_rows, source_gain)
    source_local = normed_s.shape[0]
    key_full, value_full = (
        lax.all_gather(key_weight, "tp", axis=0, tiled=True),
        lax.all_gather(value_weight, "tp", axis=0, tiled=True),
    )
    key_own = jnp.dot(normed_s, key_full, preferred_element_type=jnp.float32).astype(jnp.bfloat16)
    value_own = jnp.dot(normed_s, value_full, preferred_element_type=jnp.float32).astype(
        jnp.bfloat16
    )

    def to_slots(matrix):
        split_heads = matrix.reshape(source_local, KV_HEADS, 1, HEAD_DIM)
        spread = jnp.broadcast_to(split_heads, (source_local, KV_HEADS, copies, HEAD_DIM))
        return spread.reshape(source_local, tp_count, slot_heads * HEAD_DIM)

    key_slots, value_slots = (
        lax.all_to_all(to_slots(key_own), "tp", split_axis=1, concat_axis=0, tiled=True),
        lax.all_to_all(to_slots(value_own), "tp", split_axis=1, concat_axis=0, tiled=True),
    )
    source_block = key_slots.shape[0]
    key_flat = key_slots.reshape(source_block, slot_heads * HEAD_DIM)
    value_flat = value_slots.reshape(source_block, slot_heads * HEAD_DIM)
    pieces = lax.all_gather((normed_t, out_cotangent), "tp", axis=0, tiled=True)
    queries = jnp.dot(pieces[0], query_weight, preferred_element_type=jnp.float32).astype(
        jnp.bfloat16
    )
    d_attended = jnp.dot(pieces[1], out_weight.T, preferred_element_type=jnp.float32).astype(
        jnp.bfloat16
    )
    queries, d_attended, cotangent_block = (queries, d_attended, pieces[1])
    target_block = queries.shape[0]
    query_view = queries.reshape(target_block, slot_heads, per_slot, HEAD_DIM)
    start_state = (
        jnp.full((slot_heads, per_slot, target_block), NEGATIVE, jnp.float32),
        jnp.zeros((slot_heads, per_slot, target_block), jnp.float32),
        jnp.zeros((slot_heads, per_slot, target_block, HEAD_DIM), jnp.float32),
    )
    running = start_state
    pieces = (
        lax.all_gather(key_flat, "sp", axis=0, tiled=True),
        lax.all_gather(value_flat, "sp", axis=0, tiled=True),
    )
    length = pieces[0].shape[0]
    step_rows = 2048

    def one_block(carried, block_index):
        prior_max, prior_total, prior_sum = carried
        key_part = lax.dynamic_slice_in_dim(pieces[0], block_index * step_rows, step_rows, 0)
        value_part = lax.dynamic_slice_in_dim(pieces[1], block_index * step_rows, step_rows, 0)
        key_part = key_part.reshape(step_rows, slot_heads, HEAD_DIM)
        value_part = value_part.reshape(step_rows, slot_heads, HEAD_DIM)
        scores = (
            jnp.einsum("tgqd,sgd->gqts", query_view, key_part, preferred_element_type=jnp.float32)
            * score_scale
        )
        new_max = jnp.maximum(prior_max, jnp.max(scores, axis=-1))
        rescale = jnp.exp(prior_max - new_max)
        weights = jnp.exp(scores - new_max[..., None])
        new_total = prior_total * rescale + jnp.sum(weights, axis=-1)
        new_sum = prior_sum * rescale[..., None] + jnp.einsum(
            "gqts,sgd->gqtd",
            weights.astype(jnp.bfloat16),
            value_part,
            preferred_element_type=jnp.float32,
        )
        return ((new_max, new_total, new_sum), None)

    running, unused = lax.scan(one_block, running, jnp.arange(length // step_rows))
    row_max, total, summed = running
    attended = (
        (summed / total[..., None])
        .transpose(2, 0, 1, 3)
        .reshape(target_block, local_heads * HEAD_DIM)
        .astype(jnp.bfloat16)
    )
    log_total = (row_max + jnp.log(total)).transpose(2, 0, 1).reshape(target_block, local_heads)
    delta = jnp.sum(
        (d_attended.astype(jnp.float32) * attended.astype(jnp.float32)).reshape(
            target_block, local_heads, HEAD_DIM
        ),
        axis=-1,
    )
    all_queries, all_grads = (
        lax.all_gather(queries, "sp", axis=0, tiled=True),
        lax.all_gather(d_attended, "sp", axis=0, tiled=True),
    )
    all_logs, all_deltas = (
        lax.all_gather(log_total, "sp", axis=0, tiled=True),
        lax.all_gather(delta, "sp", axis=0, tiled=True),
    )
    whole_rows = all_queries.shape[0]
    step_rows = block_rows_for(whole_rows)
    block_shape = (whole_rows // step_rows, step_rows, slot_heads, per_slot)
    query_blocks = all_queries.reshape(block_shape + (HEAD_DIM,))
    grad_blocks = all_grads.reshape(block_shape + (HEAD_DIM,))
    log_blocks = all_logs.reshape(block_shape)
    delta_blocks = all_deltas.reshape(block_shape)

    def backward_block(sums_so_far, inputs):
        key_sum, value_sum = sums_so_far
        query_part, grad_part, log_part, delta_part = inputs
        scores = (
            jnp.einsum("tgqd,sgd->gqts", query_part, key_slots, preferred_element_type=jnp.float32)
            * score_scale
        )
        probs = jnp.exp(scores - log_part.transpose(1, 2, 0)[..., None])
        value_sum = value_sum + jnp.einsum(
            "gqts,tgqd->sgd",
            probs.astype(jnp.bfloat16),
            grad_part,
            preferred_element_type=jnp.float32,
        )
        d_probs = jnp.einsum(
            "tgqd,sgd->gqts", grad_part, value_slots, preferred_element_type=jnp.float32
        )
        d_scores = (probs * (d_probs - delta_part.transpose(1, 2, 0)[..., None])).astype(
            jnp.bfloat16
        )
        d_query = (
            jnp.einsum("gqts,sgd->tgqd", d_scores, key_slots, preferred_element_type=jnp.float32)
            * score_scale
        )
        key_sum = (
            key_sum
            + jnp.einsum("gqts,tgqd->sgd", d_scores, query_part, preferred_element_type=jnp.float32)
            * score_scale
        )
        return ((key_sum, value_sum), d_query)

    zero_sums = jnp.zeros((source_block, slot_heads, HEAD_DIM), jnp.float32)
    (key_sum, value_sum), d_query = lax.scan(
        backward_block,
        (zero_sums, zero_sums),
        (query_blocks, grad_blocks, log_blocks, delta_blocks),
    )
    query_terms = d_query.reshape(whole_rows, local_heads * HEAD_DIM)
    query_grad = lax.psum_scatter(query_terms, "sp", scatter_dimension=0, tiled=True).astype(
        jnp.bfloat16
    )
    key_back, value_back = (
        lax.all_to_all(key_sum, "tp", split_axis=0, concat_axis=1, tiled=True),
        lax.all_to_all(value_sum, "tp", split_axis=0, concat_axis=1, tiled=True),
    )

    def from_slots(matrix):
        folded = jnp.sum(matrix.reshape(source_local, KV_HEADS, copies, HEAD_DIM), axis=2)
        return folded.reshape(source_local, KV_HEADS * HEAD_DIM).astype(jnp.bfloat16)

    key_grad = from_slots(key_back)
    value_grad = from_slots(value_back)
    d_normed_s = jnp.dot(key_grad, key_full.T, preferred_element_type=jnp.float32) + jnp.dot(
        value_grad, value_full.T, preferred_element_type=jnp.float32
    )
    source_grad = norm_back(source_rows, source_gain, d_normed_s)
    d_normed_t = lax.psum_scatter(
        jnp.dot(query_grad, query_weight.T, preferred_element_type=jnp.float32),
        "tp",
        scatter_dimension=0,
        tiled=True,
    )
    target_grad = out_cotangent.astype(jnp.float32) + norm_back(
        target_rows, target_gain, d_normed_t
    )
    weight_part = jnp.dot(attended.T, cotangent_block, preferred_element_type=jnp.float32)
    out_weight_grad = lax.psum(weight_part, "sp")
    return (target_grad, source_grad, out_weight_grad)


def solution(mesh):
    return jax.shard_map(
        body,
        mesh=mesh,
        in_specs=(
            P(("sp", "tp"), None),
            P(("sp", "tp"), None),
            P(),
            P(),
            P(None, "tp"),
            P("tp", None),
            P("tp", None),
            P("tp", None),
            P(("sp", "tp"), None),
        ),
        out_specs=(P(("sp", "tp"), None), P(("sp", "tp"), None), P("tp", None)),
        check_vma=False,
    )
```

profile of v0, /device:TPU:0, one launch (start us, length us, event | category | flops | bytes accessed | tf_op | source)
XLA Modules:
  0.0 356.4 jit_solution(7738776949373914293)
XLA Ops:
  8.7 1.0 fusion.42
  10.3 1.0 fusion.44
  11.3 11.9 %all_gather.31 = bf16[192,2048]{1,0:T(8,128)(2,1)S(1)} all-gather(bf16[24,2048]{1,0:T(8,128)(2,1)S(1)} %fusion.44), channel_id=1, replica_groups=mesh['sp'=4,'tp'=8] {'tp'}, dimensions={0}, use_global_device_ids=true | all-gather | bytes 884736 | tf_op jit(solution)/shard_map/all_gather | solution.py:73
  24.3 15.0 %all_gather.32 = bf16[768,256]{1,0:T(8,128)(2,1)S(1)} all-gather(bf16[192,256]{1,0:T(8,128)(2,1)S(1)} %convolution_convert_fusion.3), channel_id=1, replica_groups=mesh['sp'=4,'tp'=8] {'sp'}, dimensions={0}, use_global_device_ids=true | all-gather | bytes 491520 | tf_op jit(solution)/shard_map/all_gather | solution.py:134
  39.5 1.2 fusion.36
  40.7 11.7 %all_gather.37 = bf16[192,2048]{1,0:T(8,128)(2,1)S(1)} all-gather(bf16[24,2048]{1,0:T(8,128)(2,1)} %param.19), channel_id=1, replica_groups=mesh['sp'=4,'tp'=8] {'tp'}, dimensions={0}, use_global_device_ids=true | all-gather | bytes 884736 | tf_op jit(solution)/shard_map/all_gather | solution.py:73
  53.0 2.1 convolution_convert_fusion.1
  55.8 3.4 all-to-all-start
  59.2 11.9 %all-gather.7.cloned.1.call-done = bf16[2048,512]{1,0:T(8,128)(2,1)} async-done(((bf16[256,512]{1,0:T(8,128)(2,1)}), bf16[2048,512]{1,0:T(8,128)(2,1)}) %all-gather.7.cloned.1.call-update) | async-done | bytes 2097168 | tf_op jit(solution)/shard_map/all_gather | solution.py:54
  71.2 2.1 convolution_convert_fusion
  74.0 3.4 all-to-all-start.1
  78.3 16.4 %all_gather.33 = bf16[4096,64]{0,1:T(8,128)(2,1)S(1)} all-gather(bf16[1024,64]{0,1:T(8,128)(2,1)S(1)} %bitcast.239), channel_id=1, replica_groups=mesh['sp'=4,'tp'=8] {'sp'}, dimensions={0}, use_global_device_ids=true | all-gather | bytes 655360 | tf_op jit(solution)/shard_map/all_gather | solution.py:90
  95.6 16.0 %all_gather.35 = bf16[4096,64]{0,1:T(8,128)(2,1)S(1)} all-gather(bf16[1024,64]{0,1:T(8,128)(2,1)S(1)} %bitcast.240), channel_id=1, replica_groups=mesh['sp'=4,'tp'=8] {'sp'}, dimensions={0}, use_global_device_ids=true | all-gather | bytes 655360 | tf_op jit(solution)/shard_map/all_gather | solution.py:91
  111.6 23.4 %while.3 = (s32[]{:T(128)}, f32[1,4,192]{2,1,0:T(4,128)S(1)}, f32[1,4,192]{2,1,0:T(4,128)S(1)}, f32[1,4,192,64]{2,3,1,0:T(8,128)S(1)}, s32[2]{0:T(128)S(1)}, /*i...) while((s32[]{:T(128)}, f32[1,4,192]{2,1,0:T(4,128)S(1)}, ...), condition=%wide.region_5.6_spmd.clone, body=%wide.region_2.5_spmd.clone.sunk | while | flops 415388160 | bytes 45173076 | solution.py:118
  112.9 4.6 %bitcast_reduce_fusion.3 = (f32[4,192]{1,0:T(4,128)S(1)}, f32[2048,192,4]{0,1,2:T(8,128)}) fusion(bf16[192,1,4,64]{0,3,2,1:T(8,128)(2,1)} %get-tuple-element.230, bf16[4096,64]{0,1:T(8,128)(2,1)S(1)} %get-tuple-element.229, s32[]{:T(128)S(6)} %select_n.6), kind=kOutput, calls=%fused_computation.1.clone.1 | convolution fusion | flops 204471552 | bytes 6654980 | tf_op jit(solution)/shard_map/while/body/eval_jaxpr/tgqd,sgd->gqts/dot_general | solution.py:103
  117.5 4.3 %fusion.90 = f32[1,4,192,64]{2,3,1,0:T(8,128)S(1)} fusion(f32[2048,192,4]{0,1,2:T(8,128)} %get-tuple-element.198, f32[4,192]{1,0:T(4,128)S(1)} %bitcast.230, f32[1,4,192,64]{2,3,1,0:T(8,128)S(1)} %get-tuple-element.215, bf16[4096,64]{0,1:T(8,128)(2,1)S(1)} %get-tuple-element.231, s32[]{:T(128)S(6)} %select_n.6, f32[4,192]{1,0:T(4,128)S(1)} %get-tuple-element.199, ...), kind=kOutput, calls=%fused_computation.8.clone.1 | convolution fusion | flops 206192640 | bytes 7020549 | tf_op jit(solution)/shard_map/while/body/eval_jaxpr/gqts,sgd->gqtd/dot_general | solution.py:110
  122.1 1.2 fusion.89
  124.6 4.6 %bitcast_reduce_fusion.3 = (f32[4,192]{1,0:T(4,128)S(1)}, f32[2048,192,4]{0,1,2:T(8,128)}) fusion(bf16[192,1,4,64]{0,3,2,1:T(8,128)(2,1)} %get-tuple-element.230, bf16[4096,64]{0,1:T(8,128)(2,1)S(1)} %get-tuple-element.229, s32[]{:T(128)S(6)} %select_n.6), kind=kOutput, calls=%fused_computation.1.clone.1 | convolution fusion | flops 204471552 | bytes 6654980 | tf_op jit(solution)/shard_map/while/body/eval_jaxpr/tgqd,sgd->gqts/dot_general | solution.py:103
  129.2 4.3 %fusion.90 = f32[1,4,192,64]{2,3,1,0:T(8,128)S(1)} fusion(f32[2048,192,4]{0,1,2:T(8,128)} %get-tuple-element.198, f32[4,192]{1,0:T(4,128)S(1)} %bitcast.230, f32[1,4,192,64]{2,3,1,0:T(8,128)S(1)} %get-tuple-element.215, bf16[4096,64]{0,1:T(8,128)(2,1)S(1)} %get-tuple-element.231, s32[]{:T(128)S(6)} %select_n.6, f32[4,192]{1,0:T(4,128)S(1)} %get-tuple-element.199, ...), kind=kOutput, calls=%fused_computation.8.clone.1 | convolution fusion | flops 206192640 | bytes 7020549 | tf_op jit(solution)/shard_map/while/body/eval_jaxpr/gqts,sgd->gqtd/dot_general | solution.py:110
  133.8 1.2 fusion.89
  135.1 1.7 convert_multiply_fusion.8
  136.9 15.1 %all_gather.38 = bf16[768,256]{1,0:T(8,128)(2,1)S(1)} all-gather(bf16[192,256]{1,0:T(8,128)(2,1)S(1)} %get-tuple-element.140), channel_id=1, replica_groups=mesh['sp'=4,'tp'=8] {'sp'}, dimensions={0}, use_global_device_ids=true | all-gather | bytes 491520 | tf_op jit(solution)/shard_map/all_gather | solution.py:135
  152.3 13.2 %all-gather.1 = f32[4,192,4]{1,2,0:T(4,128)S(1)} all-gather(f32[1,192,4]{1,2,0:T(4,128)S(1)} %bitcast.250), channel_id=1, replica_groups=mesh['sp'=4,'tp'=8] {'sp'}, dimensions={0}, use_global_device_ids=true | all-gather | bytes 15360 | tf_op jit(solution)/shard_map/all_gather | solution.py:139
  165.8 14.5 %all-gather = f32[768,1,4]{2,1,0:T(1,128)S(1)} all-gather(f32[192,1,4]{2,1,0:T(1,128)S(1)} %bitcast.247), channel_id=2, replica_groups=mesh['sp'=4,'tp'=8] {'sp'}, dimensions={0}, use_global_device_ids=true | all-gather | bytes 15360 | tf_op jit(solution)/shard_map/all_gather | solution.py:138
  180.5 2.8 fusion.54
  183.3 3.2 fusion.27
  186.5 1.3 copy-done.2
  187.8 1.2 convolution_multiply_fusion
  189.0 1.4 copy-done.3
  190.4 1.1 copy.98
  191.6 23.7 %reduce-scatter.7.cloned.1.call-done = f32[192,256]{1,0:T(8,128)} async-done(((f32[768,256]{1,0:T(8,128)}), f32[192,256]{1,0:T(8,128)}) %reduce-scatter.7.cloned.1.call-update) | async-done | bytes 196624
  215.3 1.0 copy.99
  216.3 1.7 fusion.57
  218.0 4.8 %fusion.35 = bf16[1024,1,64]{0,2,1:T(8,128)(2,1)S(1)} fusion(bf16[768,4,64]{0,2,1:T(8,128)(2,1)S(1)} %bitcast.225, bf16[4,768,1024]{1,2,0:T(8,128)(2,1)} %copy-done.3), kind=kOutput, calls=%fused_computation.43 | convolution fusion | flops 402784256 | bytes 6815744 | tf_op jit(solution)/shard_map/while/body/eval_jaxpr/gqts,tgqd->sgd/dot_general | solution.py:175
  224.2 0.9 reshape.187
  225.1 3.6 %all-to-all-start.2 = ((bf16[8,2,4096]{2,1,0:T(2,128)(2,1)}), bf16[8,2,4096]{2,1,0:T(2,128)(2,1)S(1)}, u32[]{:S(2)}, u32[]{:S(2)}) async-start(bf16[8,2,4096]{2,1,0:T(2,128)(2,1)} %reshape.187), calls=%async_computation.3 | async-start | bytes 262144 | tf_op jit(solution)/shard_map/all_to_all | solution.py:191
  228.7 6.9 %fusion.31 = bf16[1024,1,64]{0,2,1:T(8,128)(2,1)S(1)} fusion(bf16[768,4,64]{0,2,1:T(8,128)(2,1)S(1)} %bitcast.228, f32[1024,768,4]{1,0,2:T(8,128)} %copy-done.2, f32[4,768]{1,0:T(4,128)S(1)} %copy.81), kind=kOutput, calls=%fused_computation.40 | convolution fusion | flops 412090368 | bytes 13119488 | tf_op jit(solution)/shard_map/while/body/eval_jaxpr/gqts,tgqd->sgd/dot_general | solution.py:157
  237.4 4.2 %all-to-all-start.3 = ((bf16[8,2,4096]{2,1,0:T(2,128)(2,1)}), bf16[8,2,4096]{2,1,0:T(2,128)(2,1)S(1)}, u32[]{:S(2)}, u32[]{:S(2)}) async-start(bf16[8,2,4096]{2,1,0:T(2,128)(2,1)} %reshape.189), calls=%async_computation.4 | async-start | bytes 262144 | tf_op jit(solution)/shard_map/all_to_all | solution.py:192
  241.6 1.8 fusion.56
  244.2 2.9 all-to-all-done.3
  247.8 2.4 fusion.55
  250.2 2.5 fusion.41
  252.8 1.3 fusion.40
  254.1 3.6 %reduce-scatter.5.cloned.1.call-done = f32[24,2048]{1,0:T(8,128)} async-done(((f32[192,2048]{1,0:T(8,128)}), f32[24,2048]{1,0:T(8,128)}) %reduce-scatter.5.cloned.1.call-update) | async-done | bytes 196624 | tf_op jit(solution)/shard_map/reduce_scatter | solution.py:205
  257.7 1.1 fusion.48
  258.8 1.7 fusion.47
  260.5 86.2 %all-reduce.2.cloned.1.call-done = f32[256,2048]{1,0:T(8,128)} async-done(((f32[256,2048]{1,0:T(8,128)}), f32[256,2048]{1,0:T(8,128)}) %all-reduce.2.cloned.1.call-update) | async-done | bytes 2097168 | tf_op jit(solution)/shard_map/psum | solution.py:215
  346.7 3.1 copy.123
  (107 shorter events, 14.6 us)
Async XLA Ops:
  7.2 16.0 %copy-start = (bf16[2048,256]{1,0:T(8,128)(2,1)S(1)}, bf16[2048,256]{1,0:T(8,128)(2,1)}, u32[]{:S(2)}) copy-start(bf16[2048,256]{1,0:T(8,128)(2,1)} %param.15) | copy-start | bytes 3145732
  7.2 45.8 %copy-start.4 = (bf16[128,2048]{1,0:T(8,128)(2,1)S(1)}, bf16[128,2048]{1,0:T(8,128)(2,1)}, u32[]{:S(2)}) copy-start(bf16[128,2048]{1,0:T(8,128)(2,1)} %param.12) | copy-start | bytes 1572868
  7.2 45.8 %copy-start.11 = (f32[2048]{0:T(1024)S(1)}, f32[2048]{0:T(1024)}, u32[]{:S(2)}) copy-start(f32[2048]{0:T(1024)} %param.14) | copy-start | bytes 24580
  7.2 45.8 %all-gather.5.cloned.1.call-start = ((), (), s32[]{:S(2)}) async-start(), calls=%async_computation.6 | async-start | bytes 2359296 | tf_op jit(solution)/shard_map/all_gather | solution.py:53
  7.9 63.2 %all-gather.7.cloned.1.call-start = ((), (), s32[]{:S(2)}) async-start(), calls=%async_computation.7 | async-start | bytes 2359296 | tf_op jit(solution)/shard_map/all_gather | solution.py:54
  53.0 42.6 %copy-start.15 = (f32[128]{0:T(128)}, f32[128]{0:T(128)S(1)}, u32[]{:S(2)}) copy-start(f32[128]{0:T(128)S(1)} %get-tuple-element.136) | copy-start | bytes 1540
  55.8 18.2 %all-to-all-start = ((bf16[128,8,64]{0,2,1:T(8,128)(2,1)}), bf16[128,8,64]{0,2,1:T(8,128)(2,1)S(1)}, u32[]{:S(2)}, u32[]{:S(2)}) async-start(bf16[128,8,64]{0,2,1:T(8,128)(2,1)} %bitcast), calls=%async_computation | async-start | bytes 262144 | tf_op jit(solution)/shard_map/all_to_all | solution.py:67
  74.0 20.7 %all-to-all-start.1 = ((bf16[128,8,64]{0,2,1:T(8,128)(2,1)}), bf16[128,8,64]{0,2,1:T(8,128)(2,1)S(1)}, u32[]{:S(2)}, u32[]{:S(2)}) async-start(bf16[128,8,64]{0,2,1:T(8,128)(2,1)} %bitcast.7), calls=%async_computation.1 | async-start | bytes 262144 | tf_op jit(solution)/shard_map/all_to_all | solution.py:68
  77.4 137.9 %reduce-scatter.7.cloned.1.call-start = ((), (), s32[]{:S(2)}) async-start(), calls=%async_computation.10 | async-start | bytes 983040
  111.6 1.3 copy-start.17
  117.5 4.6 %copy-start.1 = (f32[2048,192,4]{0,1,2:T(8,128)S(1)}, f32[2048,192,4]{0,1,2:T(8,128)}, u32[]{:S(2)}) copy-start(f32[2048,192,4]{0,1,2:T(8,128)} %get-tuple-element.198) | copy-start | bytes 18874372 | tf_op jit(solution)/shard_map/while
  117.5 5.8 %copy-start.18 = (s32[2]{0:T(128)S(1)}, s32[2]{0:T(128)}, u32[]{:S(2)}) copy-start(s32[2]{0:T(128)} %copy-done.17) | copy-start | bytes 28 | tf_op jit(solution)/shard_map/while
  123.3 1.3 copy-start.17
  129.2 4.6 %copy-start.1 = (f32[2048,192,4]{0,1,2:T(8,128)S(1)}, f32[2048,192,4]{0,1,2:T(8,128)}, u32[]{:S(2)}) copy-start(f32[2048,192,4]{0,1,2:T(8,128)} %get-tuple-element.198) | copy-start | bytes 18874372 | tf_op jit(solution)/shard_map/while
  129.2 5.8 %copy-start.18 = (s32[2]{0:T(128)S(1)}, s32[2]{0:T(128)}, u32[]{:S(2)}) copy-start(s32[2]{0:T(128)} %copy-done.17) | copy-start | bytes 28 | tf_op jit(solution)/shard_map/while
  180.5 2.8 copy-start.8
  183.3 4.5 %copy-start.2 = (f32[1024,768,4]{1,0,2:T(8,128)}, f32[1024,768,4]{1,0,2:T(8,128)S(1)}, u32[]{:S(2)}) copy-start(f32[1024,768,4]{1,0,2:T(8,128)S(1)} %fusion.54) | copy-start | bytes 37748740
  183.3 4.5 %copy-start.7 = (bf16[1024,64,1]{0,1,2:T(8,128)(2,1)S(1)}, bf16[1024,64,1]{0,1,2:T(8,128)(2,1)}, u32[]{:S(2)}) copy-start(bf16[1024,64,1]{0,1,2:T(8,128)(2,1)} %reshape.179) | copy-start | bytes 393220
  187.8 2.6 copy-start.3
  191.5 66.2 %reduce-scatter.5.cloned.1.call-start = ((), (), s32[]{:S(2)}) async-start(), calls=%async_computation.8 | async-start | bytes 1769472 | tf_op jit(solution)/shard_map/reduce_scatter | solution.py:205
  225.1 12.3 %all-to-all-start.2 = ((bf16[8,2,4096]{2,1,0:T(2,128)(2,1)}), bf16[8,2,4096]{2,1,0:T(2,128)(2,1)S(1)}, u32[]{:S(2)}, u32[]{:S(2)}) async-start(bf16[8,2,4096]{2,1,0:T(2,128)(2,1)} %reshape.187), calls=%async_computation.3 | async-start | bytes 262144 | tf_op jit(solution)/shard_map/all_to_all | solution.py:191
  236.5 13.7 %copy-start.5 = (bf16[128,2048]{1,0:T(8,128)(2,1)S(1)}, bf16[128,2048]{1,0:T(8,128)(2,1)}, u32[]{:S(2)}) copy-start(bf16[128,2048]{1,0:T(8,128)(2,1)} %param.12) | copy-start | bytes 1572868
  236.5 13.7 %copy-start.12 = (f32[2048]{0:T(1024)S(1)}, f32[2048]{0:T(1024)}, u32[]{:S(2)}) copy-start(f32[2048]{0:T(1024)} %param.14) | copy-start | bytes 24580
  237.4 9.7 %all-to-all-start.3 = ((bf16[8,2,4096]{2,1,0:T(2,128)(2,1)}), bf16[8,2,4096]{2,1,0:T(2,128)(2,1)S(1)}, u32[]{:S(2)}, u32[]{:S(2)}) async-start(bf16[8,2,4096]{2,1,0:T(2,128)(2,1)} %reshape.189), calls=%async_computation.4 | async-start | bytes 262144 | tf_op jit(solution)/shard_map/all_to_all | solution.py:192
  241.6 105.1 %all-reduce.2.cloned.1.call-start = ((), (), s32[]{:S(2)}) async-start(), calls=%async_computation.9 | async-start | bytes 4194304 | tf_op jit(solution)/shard_map/psum | solution.py:215
  243.4 9.4 %copy-start.14 = (f32[128]{0:T(128)S(1)}, f32[128]{0:T(128)}, u32[]{:S(2)}) copy-start(f32[128]{0:T(128)} %get-tuple-element.135) | copy-start | bytes 1540
  243.4 9.4 %copy-start.16 = (f32[128]{0:T(128)S(1)}, f32[128]{0:T(128)}, u32[]{:S(2)}) copy-start(f32[128]{0:T(128)} %copy-done.15) | copy-start | bytes 1540
  244.1 13.6 %copy-start.6 = (bf16[24,2048]{1,0:T(8,128)(2,1)S(1)}, bf16[24,2048]{1,0:T(8,128)(2,1)}, u32[]{:S(2)}) copy-start(bf16[24,2048]{1,0:T(8,128)(2,1)} %param.11) | copy-start | bytes 294916
  244.1 13.6 %copy-start.10 = (f32[2048]{0:T(1024)S(1)}, f32[2048]{0:T(1024)}, u32[]{:S(2)}) copy-start(f32[2048]{0:T(1024)} %param.13) | copy-start | bytes 24580
  247.4 11.4 %copy-start.9 = (bf16[24,2048]{1,0:T(8,128)(2,1)S(1)}, bf16[24,2048]{1,0:T(8,128)(2,1)}, u32[]{:S(2)}) copy-start(bf16[24,2048]{1,0:T(8,128)(2,1)} %param.19) | copy-start | bytes 294916
  247.4 11.4 %copy-start.13 = (f32[24]{0:T(128)S(1)}, f32[24]{0:T(128)}, u32[]{:S(2)}) copy-start(f32[24]{0:T(128)} %get-tuple-element.137) | copy-start | bytes 292
Sparse Core Ops, SparseCore 0:
  9.9 30.4 all-gather.4
  42.3 28.7 all-gather.6
  191.7 23.5 reduce-scatter.6
  218.4 39.2 reduce-scatter.4
  260.5 86.1 all-reduce.1
where the time goes:
time: 358 us; the launch traced here: 356 us
  waiting for transfers between devices  130 us (36%)
  blocking collectives  114 us (32%)
  matrix products  51.2 us (14%)
  local copies, waits for them, and re-layouts  18.9 us (5%)
  starting transfers between devices  14.7 us (4%)
  between operations  14.2 us (4%)
  other arithmetic  12.3 us (3%)
    psum x1, waiting for transfers between devices, body(): out_weight_grad = lax.psum(weight_part, 'sp')  86.2 us
    unnamed x6, waiting for transfers between devices  25.1 us
    all_gather x2, blocking collectives, body(): pieces = lax.all_gather((normed_t, out_cotangent), 'tp', axis=0, tiled=True)  23.6 us
    all_gather x1, blocking collectives, body(): lax.all_gather(key_flat, 'sp', axis=0, tiled=True)  16.4 us
    all_gather x1, blocking collectives, body(): lax.all_gather(value_flat, 'sp', axis=0, tiled=True)  16 us
    all_gather x1, blocking collectives, body(): lax.all_gather(d_attended, 'sp', axis=0, tiled=True)  15.1 us
    all_gather x1, blocking collectives, body(): lax.all_gather(queries, 'sp', axis=0, tiled=True)  15 us
    all_gather x1, blocking collectives, body(): lax.all_gather(log_total, 'sp', axis=0, tiled=True)  14.5 us
  transfers between devices with their start and end apart: 9, of which 5 were waited for; matrix products, arithmetic and copies ran while one was open for 11% of the time, Pallas kernels for 0%

commit v1 on v0

v1 whole, which is shorter than its diff:
```python
import functools

import jax
import jax.numpy as jnp
from jax import lax
from jax.experimental import pallas as pl
from jax.experimental.pallas import tpu as pltpu
from jax.sharding import PartitionSpec as P

HEAD_DIM = 64
KV_HEADS = 8
EPSILON = 1e-06
MESH = pl.DeviceIdType.MESH


def normalize(matrix, gain_vector):
    widened = matrix.astype(jnp.float32)
    factor = lax.rsqrt(jnp.mean(widened * widened, axis=-1, keepdims=True) + EPSILON)
    return (widened * factor * gain_vector).astype(jnp.bfloat16)


def norm_back(matrix, gain_vector, upstream):
    widened = matrix.astype(jnp.float32)
    factor = lax.rsqrt(jnp.mean(widened * widened, axis=-1, keepdims=True) + EPSILON)
    weighted = upstream * gain_vector
    inner_sum = jnp.mean(weighted * widened, axis=-1, keepdims=True)
    return factor * weighted - widened * factor**3 * inner_sum


def exchange_kernel(kinds, sp_n, tp_n, *refs):
    count = len(kinds)
    ins, outs = refs[:count], refs[count : 2 * count]
    send_sems, recv_sems = refs[2 * count : 3 * count], refs[3 * count :]
    sp_me, tp_me = lax.axis_index("sp"), lax.axis_index("tp")
    sizes, places = {"sp": sp_n, "tp": tp_n}, {"sp": sp_me, "tp": tp_me}

    def address(axis, peer):
        return (peer, tp_me) if axis == "sp" else (sp_me, peer)

    axes = sorted({kind.split("_")[1] for kind in kinds})
    barrier = pltpu.get_barrier_semaphore()
    for axis in axes:
        for k in range(1, sizes[axis]):
            peer = lax.rem(places[axis] + k, sizes[axis])
            pl.semaphore_signal(barrier, inc=1, device_id=address(axis, peer), device_id_type=MESH)
    pl.semaphore_wait(barrier, sum(sizes[axis] - 1 for axis in axes))

    def copy(i, axis, source, slot, k, peer):
        return pltpu.make_async_remote_copy(
            src_ref=source,
            dst_ref=outs[i].at[slot],
            send_sem=send_sems[i].at[k],
            recv_sem=recv_sems[i].at[slot],
            device_id=address(axis, peer),
            device_id_type=MESH,
        )

    sent = []
    for i, kind in enumerate(kinds):
        mode, axis = kind.split("_")
        n, me = sizes[axis], places[axis]
        if mode == "pair":
            partner = me + 1 - 2 * lax.rem(me, 2)
            for k in range(1, n // 2):
                sent.append(copy(i, axis, ins[i], me, k, lax.rem(me + 2 * k, n)))
                sent[-1].start()
            sent.append(copy(i, axis, ins[i], me, 0, partner))
            sent[-1].start()
        else:
            for k in range(1, n):
                peer = lax.rem(me + k, n)
                source = ins[i] if mode == "gather" else ins[i].at[peer]
                sent.append(copy(i, axis, source, me, k, peer))
                sent[-1].start()
    for i, kind in enumerate(kinds):
        mode, axis = kind.split("_")
        me = places[axis]
        outs[i][me] = ins[i][me] if mode == "swap" else ins[i][...]
    for i, kind in enumerate(kinds):
        mode, axis = kind.split("_")
        n, me = sizes[axis], places[axis]
        if mode == "pair":
            partner = me + 1 - 2 * lax.rem(me, 2)
            for k in range(1, n // 2):
                origin = lax.rem(me + n - 2 * k, n)
                passed = copy(i, axis, outs[i].at[origin], origin, n // 2 + k - 1, partner)
                passed.wait_recv()
                passed.start()
                sent.append(passed)
    for i, kind in enumerate(kinds):
        mode, axis = kind.split("_")
        n, me = sizes[axis], places[axis]
        if mode == "pair":
            partner = me + 1 - 2 * lax.rem(me, 2)
            for k in range(n // 2):
                origin = lax.rem(partner + n - 2 * k, n)
                copy(i, axis, outs[i].at[origin], origin, 0, partner).wait_recv()
        else:
            for k in range(1, n):
                origin = lax.rem(me + n - k, n)
                copy(i, axis, outs[i].at[origin], origin, 0, origin).wait_recv()
    for one in sent:
        one.wait_send()


def exchange(collective_id, *parts):
    sp_n, tp_n = lax.axis_size("sp"), lax.axis_size("tp")
    kinds = tuple(kind for kind, array in parts)
    arrays = [array for kind, array in parts]
    shapes, sends, recvs = [], [], []
    for kind, array in parts:
        mode, axis = kind.split("_")
        n = sp_n if axis == "sp" else tp_n
        shape = array.shape if mode == "swap" else (n,) + array.shape
        shapes.append(jax.ShapeDtypeStruct(shape, array.dtype))
        sends.append(pltpu.SemaphoreType.DMA((n,)))
        recvs.append(pltpu.SemaphoreType.DMA((n,)))
    return pl.pallas_call(
        functools.partial(exchange_kernel, kinds, sp_n, tp_n),
        out_shape=shapes,
        in_specs=[pl.BlockSpec(memory_space=pltpu.VMEM)] * len(parts),
        out_specs=[pl.BlockSpec(memory_space=pltpu.VMEM)] * len(parts),
        scratch_shapes=sends + recvs,
        compiler_params=pltpu.CompilerParams(
            collective_id=collective_id,
            has_side_effects=True,
            vmem_limit_bytes=56 * 1024 * 1024,
        ),
    )(*arrays)


def matmul(left, right):
    return jnp.dot(left, right, preferred_element_type=jnp.float32)


def einsum(text, left, right):
    return jnp.einsum(text, left, right, preferred_element_type=jnp.float32)


def body(
    target_rows,
    source_rows,
    target_gain,
    source_gain,
    query_weight,
    key_weight,
    value_weight,
    out_weight,
    out_cotangent,
):
    sp_n, tp_n = lax.axis_size("sp"), lax.axis_size("tp")
    width = target_rows.shape[1]
    local_width = query_weight.shape[1]
    local_heads = local_width // HEAD_DIM
    slot_heads = max(1, KV_HEADS // tp_n)
    copies = max(1, tp_n // KV_HEADS)
    per_slot = local_heads // slot_heads
    slot_width = slot_heads * HEAD_DIM
    score_scale = HEAD_DIM ** (-0.5)
    bf16 = jnp.bfloat16

    normed_t = normalize(target_rows, target_gain)
    normed_s = normalize(source_rows, source_gain)
    source_local = normed_s.shape[0]
    target_local = normed_t.shape[0]
    target_block = tp_n * target_local
    source_block = tp_n * source_local

    rows_in, cot_in, key_full, value_full, cot_column = exchange(
        0,
        ("pair_tp", normed_t),
        ("pair_tp", out_cotangent),
        ("pair_tp", key_weight),
        ("pair_tp", value_weight),
        ("gather_sp", out_cotangent),
    )
    key_full = key_full.reshape(width, -1)
    value_full = value_full.reshape(width, -1)
    queries = matmul(rows_in.reshape(target_block, width), query_weight).astype(bf16)
    d_attended = matmul(cot_in.reshape(target_block, width), out_weight.T).astype(bf16)
    key_own = matmul(normed_s, key_full).astype(bf16)
    value_own = matmul(normed_s, value_full).astype(bf16)

    def to_slots(matrix):
        split = matrix.reshape(source_local, tp_n // copies, 1, slot_width)
        spread = jnp.broadcast_to(split, (source_local, tp_n // copies, copies, slot_width))
        return spread.reshape(source_local, tp_n, slot_width).transpose(1, 0, 2)

    slots = jnp.concatenate([to_slots(key_own), to_slots(value_own)], axis=2)
    all_queries, all_grads, kv_block, cot_all = exchange(
        1,
        ("gather_sp", queries),
        ("gather_sp", d_attended),
        ("swap_tp", slots),
        ("pair_tp", cot_column),
    )
    whole_rows = sp_n * target_block
    kv_block = kv_block.reshape(source_block, 2, slot_heads, HEAD_DIM)
    keys, values = kv_block[:, 0], kv_block[:, 1]
    head_shape = (whole_rows, slot_heads, per_slot, HEAD_DIM)
    query_view = all_queries.reshape(head_shape)
    grad_view = all_grads.reshape(head_shape)

    scores = einsum("tgqd,sgd->gqts", query_view, keys) * score_scale
    part_max = jnp.max(scores, axis=-1)
    weights = jnp.exp(scores - part_max[..., None])
    part_total = jnp.sum(weights, axis=-1)
    d_probs = einsum("tgqd,sgd->gqts", grad_view, values)
    part_delta = jnp.sum(weights * d_probs, axis=-1)
    part_sum = einsum("gqts,sgd->tgqd", weights.astype(bf16), values)
    stats = jnp.stack([part_max, part_total, part_delta]).reshape(3 * local_heads, whole_rows)
    (all_stats,) = exchange(2, ("gather_sp", stats))
    all_stats = all_stats.reshape(sp_n, 3, slot_heads, per_slot, whole_rows)
    row_max = jnp.max(all_stats[:, 0], axis=0)
    rescale = jnp.exp(all_stats[:, 0] - row_max)
    total = jnp.sum(all_stats[:, 1] * rescale, axis=0)
    delta = jnp.sum(all_stats[:, 2] * rescale, axis=0) / total
    local_scale = jnp.exp(part_max - row_max) / total

    probs = weights * local_scale[..., None]
    d_scores = (probs * (d_probs - delta[..., None])).astype(bf16)
    value_sum = einsum("gqts,tgqd->sgd", probs.astype(bf16), grad_view)
    key_sum = einsum("gqts,tgqd->sgd", d_scores, query_view) * score_scale
    d_query = einsum("gqts,sgd->tgqd", d_scores, keys) * score_scale
    d_query = d_query.reshape(sp_n, target_block, local_width).astype(bf16)
    attended_part = part_sum * local_scale.transpose(2, 0, 1)[..., None]
    attended_part = attended_part.reshape(sp_n, target_block, local_width).astype(bf16)
    grads = jnp.concatenate(
        [key_sum.reshape(source_block, slot_width), value_sum.reshape(source_block, slot_width)],
        axis=1,
    )
    grads = grads.reshape(tp_n, source_local, 2 * slot_width).astype(bf16)
    query_terms, attended_terms, grads_back = exchange(
        3, ("swap_sp", d_query), ("swap_sp", attended_part), ("swap_tp", grads)
    )
    query_grad = jnp.sum(query_terms.astype(jnp.float32), axis=0).astype(bf16)
    attended = jnp.sum(attended_terms.astype(jnp.float32), axis=0).astype(bf16)

    target_terms = matmul(query_grad, query_weight.T).astype(bf16)
    target_back, attended_all = exchange(
        4,
        ("swap_tp", target_terms.reshape(tp_n, target_local, width)),
        ("gather_sp", attended),
    )

    def from_slots(matrix):
        folded = matrix.reshape(tp_n // copies, copies, source_local, slot_width)
        folded = jnp.sum(folded.astype(jnp.float32), axis=1)
        return folded.transpose(1, 0, 2).reshape(source_local, -1).astype(bf16)

    key_grad = from_slots(grads_back[:, :, :slot_width])
    value_grad = from_slots(grads_back[:, :, slot_width:])
    d_normed_s = matmul(key_grad, key_full.T) + matmul(value_grad, value_full.T)
    source_grad = norm_back(source_rows, source_gain, d_normed_s)
    d_normed_t = jnp.sum(target_back.astype(jnp.float32), axis=0)
    target_grad = out_cotangent.astype(jnp.float32) + norm_back(
        target_rows, target_gain, d_normed_t
    )
    attended_rows = attended_all.reshape(sp_n, tp_n, target_local, local_width)
    out_weight_grad = jnp.einsum(
        "stlw,tsld->wd", attended_rows, cot_all, preferred_element_type=jnp.float32
    )
    return (target_grad, source_grad, out_weight_grad)


def solution(mesh):
    return jax.shard_map(
        body,
        mesh=mesh,
        in_specs=(
            P(("sp", "tp"), None),
            P(("sp", "tp"), None),
            P(),
            P(),
            P(None, "tp"),
            P("tp", None),
            P("tp", None),
            P("tp", None),
            P(("sp", "tp"), None),
        ),
        out_specs=(P(("sp", "tp"), None), P(("sp", "tp"), None), P("tp", None)),
        check_vma=False,
    )
```

time: 358 us -> 193 us (0.54)
  waiting for transfers between devices: 130 us -> 0 us
  Pallas kernels: 0 us -> 118 us
  blocking collectives: 114 us -> 0 us
  starting transfers between devices: 14.7 us -> 0 us
  between operations: 14.2 us -> 0.98 us
  matrix products: 51.2 us -> 39.6 us
  other arithmetic: 12.3 us -> 19 us
  local copies, waits for them, and re-layouts: 18.9 us -> 14.1 us
    pallas_call x0 -> x5, Pallas kernels: none -> 118 us  [exchange(): pl.pallas_call(functools.partial(exchange_kernel, kinds, sp_n, tp_n), out...]
    all_gather x8 -> x0, blocking collectives: 114 us -> none  [the longest x2 23.6 us: body(): pieces = lax.all_gather((normed_t, out_cotangent), 'tp', axis=0, tiled=True)]
    psum x1 -> x0, waiting for transfers between devices: 86.2 us -> none  [body(): out_weight_grad = lax.psum(weight_part, 'sp')]
    unnamed x6 -> x0, waiting for transfers between devices: 25.1 us -> none
    all_to_all x4 -> x0, starting transfers between devices: 14.5 us -> none  [the longest x1 4.16 us: body(): lax.all_to_all(value_sum, 'tp', split_axis=0, concat_axis=1, tiled=True)]
    all_gather x2 -> x0, waiting for transfers between devices: 11.9 us -> none  [the longest x1 11.9 us: body(): lax.all_gather(value_weight, 'tp', axis=0, tiled=True)]
    dot_general x17 -> x14, matrix products: 51.2 us -> 39.6 us  [the longest x6 20.6 us: einsum(): return jnp.einsum(text, left, right, preferred_element_type=jnp.float32)]
    unnamed x45 -> x18, local copies, waits for them, and re-layouts: 10.9 us -> 2.06 us
  transfers between devices with their start and end apart: 9 -> 0, of which waited for: 5 -> 0; matrix products, arithmetic and copies ran while one was open for 11% -> 0% of each run, Pallas kernels for 0% -> 0%
where the time goes in v1:
time: 193 us; the launch traced here: 192 us
  Pallas kernels  118 us (61%)
  matrix products  39.6 us (21%)
  other arithmetic  19 us (10%)
  local copies, waits for them, and re-layouts  14.1 us (7%)
    pallas_call x5, Pallas kernels, exchange(): pl.pallas_call(functools.partial(exchange_kernel, kinds, sp_n, tp_n), out...  118 us
    dot_general x6, matrix products, einsum(): return jnp.einsum(text, left, right, preferred_element_type=jnp.float32)  20.6 us
    dot_general x7, matrix products, matmul(): return jnp.dot(left, right, preferred_element_type=jnp.float32)  15.8 us
    another operation x1, other arithmetic  6.77 us
    pallas_call x4, local copies, waits for them, and re-layouts, exchange(): pl.pallas_call(functools.partial(exchange_kernel, kinds, sp_n, tp_n), out...  4.89 us

profile of v1, /device:TPU:0, one launch (start us, length us, event | category | flops | bytes accessed | tf_op | source)
XLA Modules:
  0.0 192.0 jit_solution(15663454948974413523)
XLA Ops:
  0.6 1.1 fusion.50
  1.8 1.2 fusion.44
  3.0 1.6 fusion.52.refs_0_
  4.6 44.0 %shard_map.112 = (bf16[8,24,2048]{2,1,0:T(8,128)(2,1)}, bf16[8,24,2048]{2,1,0:T(8,128)(2,1)}, bf16[8,256,512]{2,1,0:T(8,128)(2,1)}, bf16[8,256,512]{2,1,0:T(8,128)(2,1)}, bf16[4,24,2048]{2,1,0:T(8,128)(2,1)}) custom-call(bf16[24,2048]{1,0:T(8,128)(2,1)} %fusion.52.refs_0_, bf16[24,2048]{1,0:T(8,128)(2,1)} %refs_4_.1, bf16[256,512]{1,0:T(8,128)(2,1)} %refs_2_.1, ...), custom_call_target="tpu_custom_call" | custom-call | tf_op jit(solution)/shard_map/pallas_call | solution.py:118
  48.6 2.2 %convolution_convert_fusion.4.refs_0_ = bf16[192,256]{1,0:T(8,128)(2,1)} fusion(bf16[192,2048]{1,0:T(8,128)(2,1)} %bitcast.222, bf16[2048,256]{1,0:T(8,128)(2,1)S(1)} %copy-done), kind=kOutput, calls=%fused_computation.42 | convolution fusion | flops 201375744 | bytes 1933312 | tf_op jit(solution)/shard_map/dot_general | solution.py:133
  50.8 2.6 %convolution_convert_fusion.3.refs_1_ = bf16[192,256]{1,0:T(8,128)(2,1)} fusion(bf16[192,2048]{1,0:T(8,128)(2,1)} %bitcast.221, bf16[256,2048]{1,0:T(8,128)(2,1)} %param.16), kind=kOutput, calls=%fused_computation.41 | convolution fusion | flops 201375744 | bytes 1933312 | tf_op jit(solution)/shard_map/dot_general | solution.py:133
  53.4 2.3 %convolution_convert_fusion.2 = bf16[128,512]{1,0:T(8,128)(2,1)S(1)} fusion(bf16[2048,512]{1,0:T(8,128)(2,1)} %bitcast.212, bf16[128,2048]{1,0:T(8,128)(2,1)} %param.10, f32[2048]{0:T(1024)} %param.12, f32[128]{0:T(128)S(1)} %get-tuple-element.40), kind=kOutput, calls=%fused_computation.40 | convolution fusion | flops 269549568 | bytes 2761216 | tf_op jit(solution)/shard_map/dot_general | solution.py:133
  55.8 0.2 copy.30
  56.0 2.3 %convolution_convert_fusion.1 = bf16[128,512]{1,0:T(8,128)(2,1)S(1)} fusion(bf16[2048,512]{1,0:T(8,128)(2,1)} %bitcast.210, bf16[128,2048]{1,0:T(8,128)(2,1)} %param.10, f32[2048]{0:T(1024)} %param.12, f32[128]{0:T(128)S(1)} %get-tuple-element.40), kind=kOutput, calls=%fused_computation.39 | convolution fusion | flops 269549568 | bytes 2761216 | tf_op jit(solution)/shard_map/dot_general | solution.py:133
  58.4 0.2 copy.32
  58.6 0.9 pad_maximum_fusion.refs_2_
  59.4 29.8 %shard_map.113 = (bf16[4,192,256]{2,1,0:T(8,128)(2,1)}, bf16[4,192,256]{2,1,0:T(8,128)(2,1)}, bf16[8,128,128]{2,1,0:T(8,128)(2,1)}, bf16[8,4,24,2048]{3,2,1,0:T(8,128)(2,1)}) custom-call(bf16[192,256]{1,0:T(8,128)(2,1)} %convolution_convert_fusion.4.refs_0_, bf16[192,256]{1,0:T(8,128)(2,1)} %convolution_convert_fusion.3.refs_1_, ...), custom_call_target="tpu_custom_call" | custom-call | tf_op jit(solution)/shard_map/pallas_call | solution.py:118
  89.2 1.1 copy.33
  90.5 1.3 copy.35
  91.8 0.5 reshape.270
  92.2 1.3 copy.37
  93.5 0.5 reshape.272
  94.0 1.8 bitcast_reduce_fusion
  95.9 6.9 %fusion.14 = (f32[4,768]{1,0:T(4,128)S(1)}, f32[4,768]{1,0:T(4,128)S(1)}, f32[1024,768,4]{1,0,2:T(8,128)}) fusion(f32[4,768]{1,0:T(4,128)S(1)} %get-tuple-element.43, f32[1024,768,4]{1,0,2:T(8,128)S(1)} %get-tuple-element.44, bf16[768,4,64]{0,2,1:T(8,128)(2,1)S(1)} %reshape.272, bf16[1024,2,1,64]{0,3,2,1:T(8,128)(2,1)S(1)} %bitcast.207), kind=kOutput, calls=%fused_computation.16 | convolution fusion | flops 418375680 | bytes 25726976 | tf_op jit(solution)/shard_map/tgqd,sgd->gqts/dot_general | solution.py:137
  102.8 1.4 copy-done.1
  104.2 0.6 reshape.273.refs_0_
  104.8 9.1 %shard_map.114 = f32[4,12,768]{2,1,0:T(8,128)} custom-call(f32[12,768]{1,0:T(8,128)} %reshape.273.refs_0_), custom_call_target="tpu_custom_call" | custom-call | tf_op jit(solution)/shard_map/pallas_call | solution.py:118
  114.0 1.2 copy.38
  115.3 6.3 %fusion.40 = bf16[1024,1,64]{0,2,1:T(8,128)(2,1)S(1)} fusion(bf16[768,4,64]{0,2,1:T(8,128)(2,1)S(1)} %reshape.272, f32[4,768]{1,0:T(4,128)S(1)} %get-tuple-element.37, f32[4,768]{1,0:T(4,128)S(1)} %get-tuple-element.43, f32[1024,768,4]{1,0,2:T(8,128)} %copy-done.1), kind=kOutput, calls=%fused_computation.43 | convolution fusion | flops 415301632 | bytes 13131776 | tf_op jit(solution)/shard_map/gqts,tgqd->sgd/dot_general | solution.py:137
  121.7 0.6 copy-done.2
  122.3 6.8 %fusion.7 = bf16[4,768,1024]{1,2,0:T(8,128)(2,1)S(1)} fusion(f32[1024,768,4]{1,0,2:T(8,128)} %get-tuple-element.45, f32[4,768]{1,0:T(4,128)S(1)} %get-tuple-element.38, f32[4,768]{1,0:T(4,128)S(1)} %get-tuple-element.37, f32[4,768]{1,0:T(4,128)S(1)} %get-tuple-element.43, f32[1024,768,4]{1,0,2:T(8,128)S(1)} %copy-done.2), kind=kLoop, calls=%fused_computation.11 | loop fusion | flops 18874368 | bytes 31494144 | tf_op jit(solution)/shard_map/reshape.11
  129.0 2.0 %fusion.43 = bf16[1024,1,64]{0,2,1:T(8,128)(2,1)S(1)} fusion(bf16[768,4,64]{0,2,1:T(8,128)(2,1)S(1)} %reshape.270, bf16[4,768,1024]{1,2,0:T(8,128)(2,1)S(1)} %fusion.7), kind=kOutput, calls=%fused_computation.44 | convolution fusion | flops 402784256 | bytes 6815744 | tf_op jit(solution)/shard_map/gqts,tgqd->sgd/dot_general | solution.py:137
  131.0 1.2 fusion.31
  132.3 2.3 %fusion.28 = bf16[768,1,4,64]{0,3,2,1:T(8,128)(2,1)S(1)} fusion(f32[4,768]{1,0:T(4,128)S(1)} %get-tuple-element.43, f32[1024,768,4]{1,0,2:T(8,128)S(1)} %copy-done.2, f32[768,4]{0,1:T(4,128)S(1)} %bitcast.229, bf16[1024,2,1,64]{0,3,2,1:T(8,128)(2,1)S(1)} %bitcast.209), kind=kOutput, calls=%fused_computation.32 | convolution fusion | flops 412483584 | bytes 13131776 | tf_op jit(solution)/shard_map/gqts,sgd->tgqd/dot_general | solution.py:137
  134.6 0.5 convert_element_type.97
  135.0 1.1 copy.48.refs_1_
  136.1 0.5 convert_element_type.94
  136.6 1.1 copy.47.refs_0_
  137.6 0.2 copy.44
  137.8 0.2 copy.46
  138.0 0.9 pad_maximum_fusion.1.refs_2_
  138.9 21.2 %shard_map.115 = (bf16[4,192,256]{2,1,0:T(8,128)(2,1)}, bf16[4,192,256]{2,1,0:T(8,128)(2,1)}, bf16[8,128,128]{2,1,0:T(8,128)(2,1)}) custom-call(bf16[4,192,256]{2,1,0:T(8,128)(2,1)} %copy.47.refs_0_, bf16[4,192,256]{2,1,0:T(8,128)(2,1)} %copy.48.refs_1_, bf16[8,128,128]{2,1,0:T(8,128)(2,1)} %pad_maximum_fusion.1.refs_2_), custom_call_target="tpu_custom_call" | custom-call | tf_op jit(solution)/shard_map/pallas_call | solution.py:118
  160.1 1.1 reduce_sum.127
  161.2 1.7 reduce_sum.128.refs_1_
  162.9 1.2 slice_bitcast_fusion
  164.4 2.6 %fusion.68 = f32[128,2048]{1,0:T(8,128)S(1)} fusion(bf16[128,512]{0,1:T(8,128)(2,1)S(1)} %bitcast.224, bf16[2048,512]{1,0:T(8,128)(2,1)} %bitcast.213), kind=kOutput, calls=%fused_computation.89 | convolution fusion | flops 268435456 | bytes 3276800 | tf_op jit(solution)/shard_map/dot_general | solution.py:133
  166.9 2.5 %fusion.49 = (f32[128]{0:T(128)S(1)}, f32[128,2048]{1,0:T(8,128)S(1)}) fusion(bf16[128,2048]{1,0:T(8,128)(2,1)S(1)} %copy-done.3, f32[2048]{0:T(1024)S(1)} %copy-done.8, f32[128,2048]{1,0:T(8,128)S(1)} %fusion.68, bf16[128,512]{0,1:T(8,128)(2,1)S(1)} %bitcast.223, bf16[2048,512]{1,0:T(8,128)(2,1)} %bitcast.211), kind=kOutput, calls=%fused_computation.50 | convolution fusion | flops 269746048 | bytes 4858368 | tf_op jit(solution)/shard_map/dot_general | solution.py:133
  169.5 1.3 fusion.48
  170.8 1.4 convolution_convert_fusion
  172.2 14.3 %shard_map.116 = (bf16[8,24,2048]{2,1,0:T(8,128)(2,1)}, bf16[4,192,256]{2,1,0:T(8,128)(2,1)}) custom-call(bf16[8,24,2048]{2,1,0:T(8,128)(2,1)} %bitcast.205, bf16[192,256]{1,0:T(8,128)(2,1)} %reduce_sum.128.refs_1_), custom_call_target="tpu_custom_call" | custom-call | tf_op jit(solution)/shard_map/pallas_call | solution.py:118
  186.5 1.3 convert_reduce_fusion
  187.8 3.3 %fusion.17 = f32[256,2048]{1,0:T(8,128)} fusion(bf16[4,8,24,256]{3,2,1,0:T(8,128)(2,1)} %bitcast.228, bf16[8,4,24,2048]{3,2,1,0:T(8,128)(2,1)S(1)} %copy-done.4), kind=kOutput, calls=%fused_computation.19 | convolution fusion | flops 805306368 | bytes 5636096 | tf_op jit(solution)/shard_map/stlw,tsld->wd/dot_general | solution.py:260
  191.3 0.8 fusion.55
  (30 shorter events, 1.0 us)
Async XLA Ops:
  0.6 48.0 %copy-start = (bf16[2048,256]{1,0:T(8,128)(2,1)S(1)}, bf16[2048,256]{1,0:T(8,128)(2,1)}, u32[]{:S(2)}) copy-start(bf16[2048,256]{1,0:T(8,128)(2,1)} %param.13) | copy-start | bytes 3145732
  95.8 8.3 %copy-start.1 = (f32[1024,768,4]{1,0,2:T(8,128)}, f32[1024,768,4]{1,0,2:T(8,128)S(1)}, u32[]{:S(2)}) copy-start(f32[1024,768,4]{1,0,2:T(8,128)S(1)} %get-tuple-element.44) | copy-start | bytes 37748740
  114.0 8.3 %copy-start.2 = (f32[1024,768,4]{1,0,2:T(8,128)S(1)}, f32[1024,768,4]{1,0,2:T(8,128)}, u32[]{:S(2)}) copy-start(f32[1024,768,4]{1,0,2:T(8,128)} %copy-done.1) | copy-start | bytes 37748740
  132.2 34.7 %copy-start.3 = (bf16[128,2048]{1,0:T(8,128)(2,1)S(1)}, bf16[128,2048]{1,0:T(8,128)(2,1)}, u32[]{:S(2)}) copy-start(bf16[128,2048]{1,0:T(8,128)(2,1)} %param.10) | copy-start | bytes 1572868
  132.3 34.7 %copy-start.8 = (f32[2048]{0:T(1024)S(1)}, f32[2048]{0:T(1024)}, u32[]{:S(2)}) copy-start(f32[2048]{0:T(1024)} %param.12) | copy-start | bytes 24580
  137.8 53.3 %copy-start.5 = (bf16[24,2048]{1,0:T(8,128)(2,1)S(1)}, bf16[24,2048]{1,0:T(8,128)(2,1)}, u32[]{:S(2)}) copy-start(bf16[24,2048]{1,0:T(8,128)(2,1)} %param.9) | copy-start | bytes 294916
  137.8 53.3 %copy-start.7 = (f32[2048]{0:T(1024)S(1)}, f32[2048]{0:T(1024)}, u32[]{:S(2)}) copy-start(f32[2048]{0:T(1024)} %param.11) | copy-start | bytes 24580
  138.0 53.2 %copy-start.6 = (bf16[24,2048]{1,0:T(8,128)(2,1)S(1)}, bf16[24,2048]{1,0:T(8,128)(2,1)}, u32[]{:S(2)}) copy-start(bf16[24,2048]{1,0:T(8,128)(2,1)} %refs_4_.1) | copy-start | bytes 294916
  164.4 23.4 %copy-start.4 = (bf16[8,4,24,2048]{3,2,1,0:T(8,128)(2,1)S(1)}, bf16[8,4,24,2048]{3,2,1,0:T(8,128)(2,1)}, u32[]{:S(2)}) copy-start(bf16[8,4,24,2048]{3,2,1,0:T(8,128)(2,1)} %get-tuple-element.30) | copy-start | bytes 9437188

commit v2 on v1

--- a/solution.py
+++ b/solution.py
@@ -56,51 +56,152 @@
         )
 
     sent = []
+    used = [0] * count
+
+    def send(i, axis, source, target, recv, peer, keep=True):
+        one = pltpu.make_async_remote_copy(
+            src_ref=source,
+            dst_ref=target,
+            send_sem=send_sems[i].at[used[i]],
+            recv_sem=recv_sems[i].at[recv],
+            device_id=address(axis, peer),
+            device_id_type=MESH,
+        )
+        used[i] += 1
+        one.start()
+        if keep:
+            sent.append(one)
+        return one
+
+    def arrived(i, axis, target, recv):
+        pltpu.make_async_remote_copy(
+            src_ref=target,
+            dst_ref=target,
+            send_sem=send_sems[i].at[0],
+            recv_sem=recv_sems[i].at[recv],
+            device_id=address(axis, lax.rem(places[axis] + 1, sizes[axis])),
+            device_id_type=MESH,
+        ).wait_recv()
+
+    square = tp_n == 8
+    partner = tp_me + 1 - 2 * lax.rem(tp_me, 2)
+
+    def across(index):
+        return index + 2 - 4 * lax.rem(index // 2, 2)
+
+    def along(index):
+        return index + 4 - 8 * lax.rem(index // 4, 2)
+
+    def relatives(index):
+        if square:
+            return [across(index), along(index)]
+        return [lax.rem(index + 2 * k, tp_n) for k in range(1, tp_n // 2)]
+
+    def forward(i, c, origin):
+        chunks = ins[i].shape[0]
+        piece, recv = outs[i].at[origin, c], origin * chunks + c
+        arrived(i, "tp", piece, recv)
+        send(i, "tp", piece, piece, recv, partner)
+        return piece, recv
+
+    line_sent = []
+    depth = max([ins[i].shape[0] for i in range(count) if kinds[i] == "pair_tp"], default=0)
+    for c in range(depth):
+        for i, kind in enumerate(kinds):
+            if kind == "pair_tp" and c < ins[i].shape[0]:
+                chunks = ins[i].shape[0]
+                for peer in relatives(tp_me) + [partner]:
+                    piece = outs[i].at[tp_me, c]
+                    send(i, "tp", ins[i].at[c], piece, tp_me * chunks + c, peer)
+    for i, kind in enumerate(kinds):
+        mode, axis = kind.split("_")
+        n, me = sizes[axis], places[axis]
+        if mode == "line":
+            for step in (1, -1):
+                inside = (me < n - 1) if step == 1 else (me > 0)
+                line_sent.append((i, inside, used[i], me))
+
+                @pl.when(inside)
+                def _():
+                    send(i, axis, ins[i], outs[i].at[me], me, me + step, keep=False)
+        elif mode != "pair":
+            for k in range(1, n):
+                peer = lax.rem(me + k, n)
+                source = ins[i] if mode == "gather" else ins[i].at[peer]
+                send(i, axis, source, outs[i].at[me], me, peer)
+    for i, kind in enumerate(kinds):
+        mode, axis = kind.split("_")
+        me = places[axis]
+        outs[i][me] = ins[i][me] if mode == "swap" else ins[i][...]
+
+    def line_step(i, far):
+        n, me = sp_n, sp_me
+        for step in (1, -1):
+            origin = me - step * far
+            valid = (origin >= 0) if step == 1 else (origin <= n - 1)
+            onward = (valid & (me < n - 1)) if step == 1 else (valid & (me > 0))
+
+            @pl.when(valid)
+            def _():
+                arrived(i, "sp", outs[i].at[origin], origin)
+
+            if far < n - 1:
+                line_sent.append((i, onward, used[i], origin))
+
+                @pl.when(onward)
+                def _():
+                    piece = outs[i].at[origin]
+                    send(i, "sp", piece, piece, origin, me + step, keep=False)
+
+    def pair_step(i, c):
+        me = tp_me
+        chunks = ins[i].shape[0]
+        for order, origin in enumerate(relatives(me)):
+            piece, recv = forward(i, c, origin)
+            if square and order == (i + c) % 2:
+                send(i, "tp", piece, piece, recv, along(me) if order == 0 else across(me))
+
+    lines = [i for i in range(count) if kinds[i] == "line_sp"]
+    pairs = [i for i in range(count) if kinds[i] == "pair_tp"]
+    for turn in range(max(depth, sp_n - 1 if lines else 0)):
+        for i in pairs:
+            if turn < ins[i].shape[0]:
+                pair_step(i, turn)
+        for i in lines:
+            if turn + 1 < sp_n:
+                line_step(i, turn + 1)
+    if square:
+        for c in range(depth):
+            for i in pairs:
+                if c < ins[i].shape[0]:
+                    forward(i, c, across(along(tp_me)))
     for i, kind in enumerate(kinds):
         mode, axis = kind.split("_")
         n, me = sizes[axis], places[axis]
         if mode == "pair":
-            partner = me + 1 - 2 * lax.rem(me, 2)
-            for k in range(1, n // 2):
-                sent.append(copy(i, axis, ins[i], me, k, lax.rem(me + 2 * k, n)))
-                sent[-1].start()
-            sent.append(copy(i, axis, ins[i], me, 0, partner))
-            sent[-1].start()
-        else:
-            for k in range(1, n):
-                peer = lax.rem(me + k, n)
-                source = ins[i] if mode == "gather" else ins[i].at[peer]
-                sent.append(copy(i, axis, source, me, k, peer))
-                sent[-1].start()
-    for i, kind in enumerate(kinds):
-        mode, axis = kind.split("_")
-        me = places[axis]
-        outs[i][me] = ins[i][me] if mode == "swap" else ins[i][...]
-    for i, kind in enumerate(kinds):
-        mode, axis = kind.split("_")
-        n, me = sizes[axis], places[axis]
-        if mode == "pair":
-            partner = me + 1 - 2 * lax.rem(me, 2)
-            for k in range(1, n // 2):
-                origin = lax.rem(me + n - 2 * k, n)
-                passed = copy(i, axis, outs[i].at[origin], origin, n // 2 + k - 1, partner)
-                passed.wait_recv()
-                passed.start()
-                sent.append(passed)
-    for i, kind in enumerate(kinds):
-        mode, axis = kind.split("_")
-        n, me = sizes[axis], places[axis]
-        if mode == "pair":
-            partner = me + 1 - 2 * lax.rem(me, 2)
-            for k in range(n // 2):
-                origin = lax.rem(partner + n - 2 * k, n)
-                copy(i, axis, outs[i].at[origin], origin, 0, partner).wait_recv()
-        else:
+            chunks = ins[i].shape[0]
+            others = relatives(partner) + ([across(along(partner))] if square else [])
+            for origin in [partner] + others:
+                for c in range(chunks):
+                    arrived(i, axis, outs[i].at[origin, c], origin * chunks + c)
+        elif mode != "line":
             for k in range(1, n):
                 origin = lax.rem(me + n - k, n)
-                copy(i, axis, outs[i].at[origin], origin, 0, origin).wait_recv()
+                arrived(i, axis, outs[i].at[origin], origin)
     for one in sent:
         one.wait_send()
+    for i, happened, slot, origin in line_sent:
+
+        @pl.when(happened)
+        def _():
+            pltpu.make_async_remote_copy(
+                src_ref=outs[i].at[origin],
+                dst_ref=outs[i].at[origin],
+                send_sem=send_sems[i].at[slot],
+                recv_sem=recv_sems[i].at[0],
+                device_id=address("sp", lax.rem(sp_me + 1, sp_n)),
+                device_id_type=MESH,
+            ).wait_send()
 
 
 def exchange(collective_id, *parts):
@@ -113,8 +214,9 @@
         n = sp_n if axis == "sp" else tp_n
         shape = array.shape if mode == "swap" else (n,) + array.shape
         shapes.append(jax.ShapeDtypeStruct(shape, array.dtype))
-        sends.append(pltpu.SemaphoreType.DMA((n,)))
-        recvs.append(pltpu.SemaphoreType.DMA((n,)))
+        chunks = array.shape[0] if mode == "pair" else 1
+        sends.append(pltpu.SemaphoreType.DMA(((2 * n + 8) * chunks,)))
+        recvs.append(pltpu.SemaphoreType.DMA((n * chunks,)))
     return pl.pallas_call(
         functools.partial(exchange_kernel, kinds, sp_n, tp_n),
         out_shape=shapes,
@@ -166,18 +268,24 @@
     target_block = tp_n * target_local
     source_block = tp_n * source_local
 
-    rows_in, cot_in, key_full, value_full, cot_column = exchange(
+    rows_in, cot_in, cot_column = exchange(
         0,
-        ("pair_tp", normed_t),
-        ("pair_tp", out_cotangent),
-        ("pair_tp", key_weight),
-        ("pair_tp", value_weight),
-        ("gather_sp", out_cotangent),
+        ("pair_tp", normed_t[None]),
+        ("pair_tp", out_cotangent[None]),
+        ("line_sp", out_cotangent),
+    )
+    queries = matmul(rows_in.reshape(target_block, width), query_weight).astype(bf16)
+    d_attended = matmul(cot_in.reshape(target_block, width), out_weight.T).astype(bf16)
+    halves = (2, key_weight.shape[0] // 2, key_weight.shape[1])
+    key_full, value_full, all_queries, all_grads = exchange(
+        1,
+        ("pair_tp", key_weight.reshape(halves)),
+        ("pair_tp", value_weight.reshape(halves)),
+        ("line_sp", queries),
+        ("line_sp", d_attended),
     )
     key_full = key_full.reshape(width, -1)
     value_full = value_full.reshape(width, -1)
-    queries = matmul(rows_in.reshape(target_block, width), query_weight).astype(bf16)
-    d_attended = matmul(cot_in.reshape(target_block, width), out_weight.T).astype(bf16)
     key_own = matmul(normed_s, key_full).astype(bf16)
     value_own = matmul(normed_s, value_full).astype(bf16)
 
@@ -187,13 +295,7 @@
         return spread.reshape(source_local, tp_n, slot_width).transpose(1, 0, 2)
 
     slots = jnp.concatenate([to_slots(key_own), to_slots(value_own)], axis=2)
-    all_queries, all_grads, kv_block, cot_all = exchange(
-        1,
-        ("gather_sp", queries),
-        ("gather_sp", d_attended),
-        ("swap_tp", slots),
-        ("pair_tp", cot_column),
-    )
+    (kv_block,) = exchange(2, ("swap_tp", slots))
     whole_rows = sp_n * target_block
     kv_block = kv_block.reshape(source_block, 2, slot_heads, HEAD_DIM)
     keys, values = kv_block[:, 0], kv_block[:, 1]
@@ -209,7 +311,7 @@
     part_delta = jnp.sum(weights * d_probs, axis=-1)
     part_sum = einsum("gqts,sgd->tgqd", weights.astype(bf16), values)
     stats = jnp.stack([part_max, part_total, part_delta]).reshape(3 * local_heads, whole_rows)
-    (all_stats,) = exchange(2, ("gather_sp", stats))
+    (all_stats,) = exchange(3, ("gather_sp", stats))
     all_stats = all_stats.reshape(sp_n, 3, slot_heads, per_slot, whole_rows)
     row_max = jnp.max(all_stats[:, 0], axis=0)
     rescale = jnp.exp(all_stats[:, 0] - row_max)
@@ -230,17 +332,21 @@
         axis=1,
     )
     grads = grads.reshape(tp_n, source_local, 2 * slot_width).astype(bf16)
-    query_terms, attended_terms, grads_back = exchange(
-        3, ("swap_sp", d_query), ("swap_sp", attended_part), ("swap_tp", grads)
+    query_terms, attended_terms, grads_back, cot_all = exchange(
+        4,
+        ("swap_sp", d_query),
+        ("swap_sp", attended_part),
+        ("swap_tp", grads),
+        ("pair_tp", cot_column),
     )
     query_grad = jnp.sum(query_terms.astype(jnp.float32), axis=0).astype(bf16)
     attended = jnp.sum(attended_terms.astype(jnp.float32), axis=0).astype(bf16)
 
     target_terms = matmul(query_grad, query_weight.T).astype(bf16)
     target_back, attended_all = exchange(
-        4,
+        5,
         ("swap_tp", target_terms.reshape(tp_n, target_local, width)),
-        ("gather_sp", attended),
+        ("line_sp", attended),
     )
 
     def from_slots(matrix):

time: 193 us -> 183 us (0.948)
  Pallas kernels: 118 us -> 109 us
    pallas_call x5 -> x6, Pallas kernels: 118 us -> 109 us  [exchange(): pl.pallas_call(functools.partial(exchange_kernel, kinds, sp_n, tp_n), out...]
where the time goes in v2:
time: 183 us; the launch traced here: 182 us
  Pallas kernels  109 us (60%)
  matrix products  39.7 us (22%)
  other arithmetic  19 us (10%)
  local copies, waits for them, and re-layouts  14 us (8%)
    pallas_call x6, Pallas kernels, exchange(): pl.pallas_call(functools.partial(exchange_kernel, kinds, sp_n, tp_n), out...  109 us
    dot_general x6, matrix products, einsum(): return jnp.einsum(text, left, right, preferred_element_type=jnp.float32)  20.6 us
    dot_general x7, matrix products, matmul(): return jnp.dot(left, right, preferred_element_type=jnp.float32)  15.8 us
    another operation x1, other arithmetic  6.77 us
    pallas_call x4, local copies, waits for them, and re-layouts, exchange(): pl.pallas_call(functools.partial(exchange_kernel, kinds, sp_n, tp_n), out...  4.89 us

profile of v2, /device:TPU:0, one launch (start us, length us, event | category | flops | bytes accessed | tf_op | source)
XLA Modules:
  0.0 182.2 jit_solution(3243654477202634121)
XLA Ops:
  0.6 1.1 fusion.50
  1.8 1.2 fusion.44
  3.0 1.6 fusion.61.refs_0_
  4.6 22.8 %shard_map.112 = (bf16[8,1,24,2048]{3,2,1,0:T(8,128)(2,1)}, bf16[8,1,24,2048]{3,2,1,0:T(8,128)(2,1)}, bf16[4,24,2048]{2,1,0:T(8,128)(2,1)}) custom-call(bf16[1,24,2048]{2,1,0:T(8,128)(2,1)} %fusion.61.refs_0_, bf16[1,24,2048]{2,1,0:T(8,128)(2,1)} %bitcast.223, bf16[24,2048]{1,0:T(8,128)(2,1)} %refs_2_.1), custom_call_target="tpu_custom_call" | custom-call | tf_op jit(solution)/shard_map/pallas_call | solution.py:220
  27.5 2.2 %convolution_convert_fusion.4.refs_2_ = bf16[192,256]{1,0:T(8,128)(2,1)} fusion(bf16[192,2048]{1,0:T(8,128)(2,1)} %bitcast.228, bf16[2048,256]{1,0:T(8,128)(2,1)S(1)} %copy-done), kind=kOutput, calls=%fused_computation.42 | convolution fusion | flops 201375744 | bytes 1933312 | tf_op jit(solution)/shard_map/dot_general | solution.py:235
  29.6 2.6 %convolution_convert_fusion.3.refs_3_ = bf16[192,256]{1,0:T(8,128)(2,1)} fusion(bf16[192,2048]{1,0:T(8,128)(2,1)} %bitcast.227, bf16[256,2048]{1,0:T(8,128)(2,1)} %param.16), kind=kOutput, calls=%fused_computation.41 | convolution fusion | flops 201375744 | bytes 1933312 | tf_op jit(solution)/shard_map/dot_general | solution.py:235
  32.2 27.5 %shard_map.113 = (bf16[8,2,128,512]{3,2,1,0:T(8,128)(2,1)}, bf16[8,2,128,512]{3,2,1,0:T(8,128)(2,1)}, bf16[4,192,256]{2,1,0:T(8,128)(2,1)}, bf16[4,192,256]{2,1,0:T(8,128)(2,1)}) custom-call(bf16[2,128,512]{2,1,0:T(8,128)(2,1)} %bitcast.235, bf16[2,128,512]{2,1,0:T(8,128)(2,1)} %bitcast.236, bf16[192,256]{1,0:T(8,128)(2,1)} %convolution_convert_fusion.4.refs_2_, ...), custom_call_target="tpu_custom_call" | custom-call | tf_op jit(solution)/shard_map/pallas_call | solution.py:220
  59.8 2.3 %convolution_convert_fusion.1 = bf16[128,512]{1,0:T(8,128)(2,1)S(1)} fusion(bf16[2048,512]{1,0:T(8,128)(2,1)} %bitcast.215, bf16[128,2048]{1,0:T(8,128)(2,1)} %param.10, f32[2048]{0:T(1024)} %param.12, f32[128]{0:T(128)S(1)} %get-tuple-element.38), kind=kOutput, calls=%fused_computation.39 | convolution fusion | flops 269549568 | bytes 2761216 | tf_op jit(solution)/shard_map/dot_general | solution.py:235
  62.2 0.2 copy.32
  62.4 2.3 %convolution_convert_fusion.2 = bf16[128,512]{1,0:T(8,128)(2,1)S(1)} fusion(bf16[2048,512]{1,0:T(8,128)(2,1)} %bitcast.217, bf16[128,2048]{1,0:T(8,128)(2,1)} %param.10, f32[2048]{0:T(1024)} %param.12, f32[128]{0:T(128)S(1)} %get-tuple-element.38), kind=kOutput, calls=%fused_computation.40 | convolution fusion | flops 269549568 | bytes 2761216 | tf_op jit(solution)/shard_map/dot_general | solution.py:235
  64.8 0.2 copy.30
  65.0 0.9 pad_maximum_fusion.refs_0_
  65.8 7.4 %shard_map.114 = bf16[8,128,128]{2,1,0:T(8,128)(2,1)} custom-call(bf16[8,128,128]{2,1,0:T(8,128)(2,1)} %pad_maximum_fusion.refs_0_), custom_call_target="tpu_custom_call" | custom-call | tf_op jit(solution)/shard_map/pallas_call | solution.py:220
  73.3 1.1 copy.33
  74.5 1.3 copy.35
  75.8 0.5 reshape.278
  76.3 1.3 copy.37
  77.6 0.5 reshape.280
  78.0 1.8 %bitcast_reduce_fusion = (f32[4,768]{1,0:T(4,128)S(1)}, f32[1024,768,4]{1,0,2:T(8,128)S(1)}) fusion(bf16[768,4,64]{0,2,1:T(8,128)(2,1)S(1)} %reshape.278, bf16[1024,2,1,64]{0,3,2,1:T(8,128)(2,1)S(1)} %bitcast.211), kind=kOutput, calls=%fused_computation.6 | convolution fusion | flops 408941568 | bytes 13119488 | tf_op jit(solution)/shard_map/tgqd,sgd->gqts/dot_general | solution.py:239
  79.9 7.0 %fusion.14 = (f32[4,768]{1,0:T(4,128)S(1)}, f32[4,768]{1,0:T(4,128)S(1)}, f32[1024,768,4]{1,0,2:T(8,128)}) fusion(f32[4,768]{1,0:T(4,128)S(1)} %get-tuple-element.41, f32[1024,768,4]{1,0,2:T(8,128)S(1)} %get-tuple-element.42, bf16[768,4,64]{0,2,1:T(8,128)(2,1)S(1)} %reshape.280, bf16[1024,2,1,64]{0,3,2,1:T(8,128)(2,1)S(1)} %bitcast.212), kind=kOutput, calls=%fused_computation.16 | convolution fusion | flops 418375680 | bytes 25726976 | tf_op jit(solution)/shard_map/tgqd,sgd->gqts/dot_general | solution.py:239
  86.9 1.4 copy-done.1
  88.2 0.6 reshape.281.refs_0_
  88.9 9.1 %shard_map.115 = f32[4,12,768]{2,1,0:T(8,128)} custom-call(f32[12,768]{1,0:T(8,128)} %reshape.281.refs_0_), custom_call_target="tpu_custom_call" | custom-call | tf_op jit(solution)/shard_map/pallas_call | solution.py:220
  98.0 1.2 copy.38
  99.3 6.3 %fusion.40 = bf16[1024,1,64]{0,2,1:T(8,128)(2,1)S(1)} fusion(bf16[768,4,64]{0,2,1:T(8,128)(2,1)S(1)} %reshape.280, f32[4,768]{1,0:T(4,128)S(1)} %get-tuple-element.35, f32[4,768]{1,0:T(4,128)S(1)} %get-tuple-element.41, f32[1024,768,4]{1,0,2:T(8,128)} %copy-done.1), kind=kOutput, calls=%fused_computation.43 | convolution fusion | flops 415301632 | bytes 13131776 | tf_op jit(solution)/shard_map/gqts,tgqd->sgd/dot_general | solution.py:239
  105.7 0.6 copy-done.2
  106.3 6.8 %fusion.7 = bf16[4,768,1024]{1,2,0:T(8,128)(2,1)S(1)} fusion(f32[1024,768,4]{1,0,2:T(8,128)} %get-tuple-element.43, f32[4,768]{1,0:T(4,128)S(1)} %get-tuple-element.36, f32[4,768]{1,0:T(4,128)S(1)} %get-tuple-element.35, f32[4,768]{1,0:T(4,128)S(1)} %get-tuple-element.41, f32[1024,768,4]{1,0,2:T(8,128)S(1)} %copy-done.2), kind=kLoop, calls=%fused_computation.11 | loop fusion | flops 18874368 | bytes 31494144 | tf_op jit(solution)/shard_map/reshape.11
  113.0 2.0 %fusion.43 = bf16[1024,1,64]{0,2,1:T(8,128)(2,1)S(1)} fusion(bf16[768,4,64]{0,2,1:T(8,128)(2,1)S(1)} %reshape.278, bf16[4,768,1024]{1,2,0:T(8,128)(2,1)S(1)} %fusion.7), kind=kOutput, calls=%fused_computation.44 | convolution fusion | flops 402784256 | bytes 6815744 | tf_op jit(solution)/shard_map/gqts,tgqd->sgd/dot_general | solution.py:239
  115.0 1.2 fusion.31
  116.3 2.3 %fusion.28 = bf16[768,1,4,64]{0,3,2,1:T(8,128)(2,1)S(1)} fusion(f32[4,768]{1,0:T(4,128)S(1)} %get-tuple-element.41, f32[1024,768,4]{1,0,2:T(8,128)S(1)} %copy-done.2, f32[768,4]{0,1:T(4,128)S(1)} %bitcast.237, bf16[1024,2,1,64]{0,3,2,1:T(8,128)(2,1)S(1)} %bitcast.214), kind=kOutput, calls=%fused_computation.32 | convolution fusion | flops 412483584 | bytes 13131776 | tf_op jit(solution)/shard_map/gqts,sgd->tgqd/dot_general | solution.py:239
  118.6 0.5 convert_element_type.97
  119.0 1.1 copy.48.refs_1_
  120.1 0.5 convert_element_type.94
  120.6 1.1 copy.47.refs_0_
  121.8 0.2 copy.46
  122.0 0.9 pad_maximum_fusion.1.refs_2_
  122.9 25.5 %shard_map.116 = (bf16[4,192,256]{2,1,0:T(8,128)(2,1)}, bf16[4,192,256]{2,1,0:T(8,128)(2,1)}, bf16[8,128,128]{2,1,0:T(8,128)(2,1)}, bf16[8,4,24,2048]{3,2,1,0:T(8,128)(2,1)}) custom-call(bf16[4,192,256]{2,1,0:T(8,128)(2,1)} %copy.47.refs_0_, bf16[4,192,256]{2,1,0:T(8,128)(2,1)} %copy.48.refs_1_, bf16[8,128,128]{2,1,0:T(8,128)(2,1)} %pad_maximum_fusion.1.refs_2_, ...), custom_call_target="tpu_custom_call" | custom-call | tf_op jit(solution)/shard_map/pallas_call | solution.py:220
  148.4 1.1 reduce_sum.127
  149.4 1.7 reduce_sum.128.refs_1_
  151.1 1.2 slice_bitcast_fusion
  152.6 2.6 %fusion.69 = f32[128,2048]{1,0:T(8,128)S(1)} fusion(bf16[128,512]{0,1:T(8,128)(2,1)S(1)} %bitcast.230, bf16[2048,512]{1,0:T(8,128)(2,1)} %bitcast.218), kind=kOutput, calls=%fused_computation.90 | convolution fusion | flops 268435456 | bytes 3276800 | tf_op jit(solution)/shard_map/dot_general | solution.py:235
  155.2 2.5 %fusion.49 = (f32[128]{0:T(128)S(1)}, f32[128,2048]{1,0:T(8,128)S(1)}) fusion(bf16[128,2048]{1,0:T(8,128)(2,1)S(1)} %copy-done.3, f32[2048]{0:T(1024)S(1)} %copy-done.8, f32[128,2048]{1,0:T(8,128)S(1)} %fusion.69, bf16[128,512]{0,1:T(8,128)(2,1)S(1)} %bitcast.229, bf16[2048,512]{1,0:T(8,128)(2,1)} %bitcast.216), kind=kOutput, calls=%fused_computation.50 | convolution fusion | flops 269746048 | bytes 4858368 | tf_op jit(solution)/shard_map/dot_general | solution.py:235
  157.7 1.3 fusion.48
  159.1 1.4 convolution_convert_fusion
  160.4 16.2 %shard_map.117 = (bf16[8,24,2048]{2,1,0:T(8,128)(2,1)}, bf16[4,192,256]{2,1,0:T(8,128)(2,1)}) custom-call(bf16[8,24,2048]{2,1,0:T(8,128)(2,1)} %bitcast.210, bf16[192,256]{1,0:T(8,128)(2,1)} %reduce_sum.128.refs_1_), custom_call_target="tpu_custom_call" | custom-call | tf_op jit(solution)/shard_map/pallas_call | solution.py:220
  176.7 1.3 convert_reduce_fusion
  178.0 3.3 %fusion.17 = f32[256,2048]{1,0:T(8,128)} fusion(bf16[4,8,24,256]{3,2,1,0:T(8,128)(2,1)} %bitcast.234, bf16[8,4,24,2048]{3,2,1,0:T(8,128)(2,1)S(1)} %copy-done.4), kind=kOutput, calls=%fused_computation.19 | convolution fusion | flops 805306368 | bytes 5636096 | tf_op jit(solution)/shard_map/stlw,tsld->wd/dot_general | solution.py:366
  181.4 0.8 fusion.55
  (31 shorter events, 1.2 us)
Async XLA Ops:
  0.6 26.8 %copy-start = (bf16[2048,256]{1,0:T(8,128)(2,1)S(1)}, bf16[2048,256]{1,0:T(8,128)(2,1)}, u32[]{:S(2)}) copy-start(bf16[2048,256]{1,0:T(8,128)(2,1)} %param.13) | copy-start | bytes 3145732
  79.9 8.3 %copy-start.1 = (f32[1024,768,4]{1,0,2:T(8,128)}, f32[1024,768,4]{1,0,2:T(8,128)S(1)}, u32[]{:S(2)}) copy-start(f32[1024,768,4]{1,0,2:T(8,128)S(1)} %get-tuple-element.42) | copy-start | bytes 37748740
  98.0 8.3 %copy-start.2 = (f32[1024,768,4]{1,0,2:T(8,128)S(1)}, f32[1024,768,4]{1,0,2:T(8,128)}, u32[]{:S(2)}) copy-start(f32[1024,768,4]{1,0,2:T(8,128)} %copy-done.1) | copy-start | bytes 37748740
  116.2 38.9 %copy-start.3 = (bf16[128,2048]{1,0:T(8,128)(2,1)S(1)}, bf16[128,2048]{1,0:T(8,128)(2,1)}, u32[]{:S(2)}) copy-start(bf16[128,2048]{1,0:T(8,128)(2,1)} %param.10) | copy-start | bytes 1572868
  116.3 38.9 %copy-start.8 = (f32[2048]{0:T(1024)S(1)}, f32[2048]{0:T(1024)}, u32[]{:S(2)}) copy-start(f32[2048]{0:T(1024)} %param.12) | copy-start | bytes 24580
  122.0 59.3 %copy-start.5 = (bf16[24,2048]{1,0:T(8,128)(2,1)S(1)}, bf16[24,2048]{1,0:T(8,128)(2,1)}, u32[]{:S(2)}) copy-start(bf16[24,2048]{1,0:T(8,128)(2,1)} %param.9) | copy-start | bytes 294916
  122.0 59.3 %copy-start.7 = (f32[2048]{0:T(1024)S(1)}, f32[2048]{0:T(1024)}, u32[]{:S(2)}) copy-start(f32[2048]{0:T(1024)} %param.11) | copy-start | bytes 24580
  122.9 58.5 %copy-start.6 = (bf16[24,2048]{1,0:T(8,128)(2,1)S(1)}, bf16[24,2048]{1,0:T(8,128)(2,1)}, u32[]{:S(2)}) copy-start(bf16[24,2048]{1,0:T(8,128)(2,1)} %refs_2_.1) | copy-start | bytes 294916
  152.6 25.4 %copy-start.4 = (bf16[8,4,24,2048]{3,2,1,0:T(8,128)(2,1)S(1)}, bf16[8,4,24,2048]{3,2,1,0:T(8,128)(2,1)}, u32[]{:S(2)}) copy-start(bf16[8,4,24,2048]{3,2,1,0:T(8,128)(2,1)} %get-tuple-element.28) | copy-start | bytes 9437188

commit v3 on v2

--- a/solution.py
+++ b/solution.py
@@ -119,11 +119,14 @@
         if mode == "line":
             for step in (1, -1):
                 inside = (me < n - 1) if step == 1 else (me > 0)
-                line_sent.append((i, inside, used[i], me))
-
-                @pl.when(inside)
-                def _():
-                    send(i, axis, ins[i], outs[i].at[me], me, me + step, keep=False)
+                for c in range(ins[i].shape[0]):
+                    line_sent.append((i, inside, used[i], me, c))
+                    recv = me * ins[i].shape[0] + c
+
+                    @pl.when(inside)
+                    def _():
+                        piece = outs[i].at[me, c]
+                        send(i, axis, ins[i].at[c], piece, recv, me + step, keep=False)
         elif mode != "pair":
             for k in range(1, n):
                 peer = lax.rem(me + k, n)
@@ -134,8 +137,9 @@
         me = places[axis]
         outs[i][me] = ins[i][me] if mode == "swap" else ins[i][...]
 
-    def line_step(i, far):
+    def line_step(i, far, c):
         n, me = sp_n, sp_me
+        chunks = ins[i].shape[0]
         for step in (1, -1):
             origin = me - step * far
             valid = (origin >= 0) if step == 1 else (origin <= n - 1)
@@ -143,15 +147,16 @@
 
             @pl.when(valid)
             def _():
-                arrived(i, "sp", outs[i].at[origin], origin)
+                arrived(i, "sp", outs[i].at[origin, c], origin * chunks + c)
 
             if far < n - 1:
-                line_sent.append((i, onward, used[i], origin))
+                line_sent.append((i, onward, used[i], origin, c))
 
                 @pl.when(onward)
                 def _():
-                    piece = outs[i].at[origin]
-                    send(i, "sp", piece, piece, origin, me + step, keep=False)
+                    piece = outs[i].at[origin, c]
+                    recv = origin * chunks + c
+                    send(i, "sp", piece, piece, recv, me + step, keep=False)
 
     def pair_step(i, c):
         me = tp_me
@@ -169,7 +174,8 @@
                 pair_step(i, turn)
         for i in lines:
             if turn + 1 < sp_n:
-                line_step(i, turn + 1)
+                for c in range(ins[i].shape[0]):
+                    line_step(i, turn + 1, c)
     if square:
         for c in range(depth):
             for i in pairs:
@@ -190,13 +196,13 @@
                 arrived(i, axis, outs[i].at[origin], origin)
     for one in sent:
         one.wait_send()
-    for i, happened, slot, origin in line_sent:
+    for i, happened, slot, origin, c in line_sent:
 
         @pl.when(happened)
         def _():
             pltpu.make_async_remote_copy(
-                src_ref=outs[i].at[origin],
-                dst_ref=outs[i].at[origin],
+                src_ref=outs[i].at[origin, c],
+                dst_ref=outs[i].at[origin, c],
                 send_sem=send_sems[i].at[slot],
                 recv_sem=recv_sems[i].at[0],
                 device_id=address("sp", lax.rem(sp_me + 1, sp_n)),
@@ -214,7 +220,7 @@
         n = sp_n if axis == "sp" else tp_n
         shape = array.shape if mode == "swap" else (n,) + array.shape
         shapes.append(jax.ShapeDtypeStruct(shape, array.dtype))
-        chunks = array.shape[0] if mode == "pair" else 1
+        chunks = array.shape[0] if mode in ("pair", "line") else 1
         sends.append(pltpu.SemaphoreType.DMA(((2 * n + 8) * chunks,)))
         recvs.append(pltpu.SemaphoreType.DMA((n * chunks,)))
     return pl.pallas_call(
@@ -268,21 +274,22 @@
     target_block = tp_n * target_local
     source_block = tp_n * source_local
 
-    rows_in, cot_in, cot_column = exchange(
+    rows_in, cot_in = exchange(
         0,
         ("pair_tp", normed_t[None]),
         ("pair_tp", out_cotangent[None]),
-        ("line_sp", out_cotangent),
     )
     queries = matmul(rows_in.reshape(target_block, width), query_weight).astype(bf16)
     d_attended = matmul(cot_in.reshape(target_block, width), out_weight.T).astype(bf16)
     halves = (2, key_weight.shape[0] // 2, key_weight.shape[1])
-    key_full, value_full, all_queries, all_grads = exchange(
+    split = (2, target_block // 2, local_width)
+    key_full, value_full, all_queries, all_grads, cot_column = exchange(
         1,
         ("pair_tp", key_weight.reshape(halves)),
         ("pair_tp", value_weight.reshape(halves)),
-        ("line_sp", queries),
-        ("line_sp", d_attended),
+        ("line_sp", queries.reshape(split)),
+        ("line_sp", d_attended.reshape(split)),
+        ("line_sp", out_cotangent[None]),
     )
     key_full = key_full.reshape(width, -1)
     value_full = value_full.reshape(width, -1)
@@ -319,14 +326,14 @@
     delta = jnp.sum(all_stats[:, 2] * rescale, axis=0) / total
     local_scale = jnp.exp(part_max - row_max) / total
 
+    attended_part = part_sum * local_scale.transpose(2, 0, 1)[..., None]
+    attended_part = attended_part.reshape(sp_n, target_block, local_width).astype(bf16)
     probs = weights * local_scale[..., None]
     d_scores = (probs * (d_probs - delta[..., None])).astype(bf16)
     value_sum = einsum("gqts,tgqd->sgd", probs.astype(bf16), grad_view)
     key_sum = einsum("gqts,tgqd->sgd", d_scores, query_view) * score_scale
     d_query = einsum("gqts,sgd->tgqd", d_scores, keys) * score_scale
     d_query = d_query.reshape(sp_n, target_block, local_width).astype(bf16)
-    attended_part = part_sum * local_scale.transpose(2, 0, 1)[..., None]
-    attended_part = attended_part.reshape(sp_n, target_block, local_width).astype(bf16)
     grads = jnp.concatenate(
         [key_sum.reshape(source_block, slot_width), value_sum.reshape(source_block, slot_width)],
         axis=1,
@@ -337,7 +344,7 @@
         ("swap_sp", d_query),
         ("swap_sp", attended_part),
         ("swap_tp", grads),
-        ("pair_tp", cot_column),
+        ("pair_tp", cot_column.reshape(sp_n, target_local, width)),
     )
     query_grad = jnp.sum(query_terms.astype(jnp.float32), axis=0).astype(bf16)
     attended = jnp.sum(attended_terms.astype(jnp.float32), axis=0).astype(bf16)
@@ -346,7 +353,7 @@
     target_back, attended_all = exchange(
         5,
         ("swap_tp", target_terms.reshape(tp_n, target_local, width)),
-        ("line_sp", attended),
+        ("line_sp", attended.reshape(split)),
     )
 
     def from_slots(matrix):

time: 183 us -> 182 us (level)
  Pallas kernels: 109 us -> 107 us
where the time goes in v3:
time: 182 us; the launch traced here: 181 us
  Pallas kernels  107 us (59%)
  matrix products  39.7 us (22%)
  other arithmetic  19 us (10%)
  local copies, waits for them, and re-layouts  14 us (8%)
    pallas_call x6, Pallas kernels, exchange(): pl.pallas_call(functools.partial(exchange_kernel, kinds, sp_n, tp_n), out...  107 us
    dot_general x6, matrix products, einsum(): return jnp.einsum(text, left, right, preferred_element_type=jnp.float32)  20.6 us
    dot_general x7, matrix products, matmul(): return jnp.dot(left, right, preferred_element_type=jnp.float32)  15.8 us
    another operation x1, other arithmetic  6.77 us
    pallas_call x4, local copies, waits for them, and re-layouts, exchange(): pl.pallas_call(functools.partial(exchange_kernel, kinds, sp_n, tp_n), out...  4.91 us

profile of v3, /device:TPU:0, one launch (start us, length us, event | category | flops | bytes accessed | tf_op | source)
XLA Modules:
  0.0 180.8 jit_solution(7068406512579299944)
XLA Ops:
  0.6 1.1 fusion.50
  1.8 1.2 fusion.44
  3.0 1.6 fusion.61.refs_0_
  4.6 17.3 %shard_map.112 = (bf16[8,1,24,2048]{3,2,1,0:T(8,128)(2,1)}, bf16[8,1,24,2048]{3,2,1,0:T(8,128)(2,1)}) custom-call(bf16[1,24,2048]{2,1,0:T(8,128)(2,1)} %fusion.61.refs_0_, bf16[1,24,2048]{2,1,0:T(8,128)(2,1)} %bitcast.227), custom_call_target="tpu_custom_call" | custom-call | tf_op jit(solution)/shard_map/pallas_call | solution.py:226
  22.0 2.2 %convolution_convert_fusion.4 = bf16[192,256]{1,0:T(8,128)(2,1)} fusion(bf16[192,2048]{1,0:T(8,128)(2,1)} %bitcast.233, bf16[2048,256]{1,0:T(8,128)(2,1)S(1)} %copy-done), kind=kOutput, calls=%fused_computation.42 | convolution fusion | flops 201375744 | bytes 1933312 | tf_op jit(solution)/shard_map/dot_general | solution.py:241
  24.1 2.6 %convolution_convert_fusion.3 = bf16[192,256]{1,0:T(8,128)(2,1)} fusion(bf16[192,2048]{1,0:T(8,128)(2,1)} %bitcast.232, bf16[256,2048]{1,0:T(8,128)(2,1)} %param.16), kind=kOutput, calls=%fused_computation.41 | convolution fusion | flops 201375744 | bytes 1933312 | tf_op jit(solution)/shard_map/dot_general | solution.py:241
  26.8 31.9 %shard_map.113 = (bf16[8,2,128,512]{3,2,1,0:T(8,128)(2,1)}, bf16[8,2,128,512]{3,2,1,0:T(8,128)(2,1)}, bf16[4,2,96,256]{3,2,1,0:T(8,128)(2,1)}, bf16[4,2,96,256]{3,2,1,0:T(8,128)(2,1)}, bf16[4,1,24,2048]{3,2,1,0:T(8,128)(2,1)}) custom-call(bf16[2,128,512]{2,1,0:T(8,128)(2,1)} %bitcast.244, bf16[2,128,512]{2,1,0:T(8,128)(2,1)} %bitcast.245, ...), custom_call_target="tpu_custom_call" | custom-call | tf_op jit(solution)/shard_map/pallas_call | solution.py:226
  58.7 2.3 %convolution_convert_fusion.1 = bf16[128,512]{1,0:T(8,128)(2,1)S(1)} fusion(bf16[2048,512]{1,0:T(8,128)(2,1)} %bitcast.219, bf16[128,2048]{1,0:T(8,128)(2,1)} %param.10, f32[2048]{0:T(1024)} %param.12, f32[128]{0:T(128)S(1)} %get-tuple-element.38), kind=kOutput, calls=%fused_computation.39 | convolution fusion | flops 269549568 | bytes 2761216 | tf_op jit(solution)/shard_map/dot_general | solution.py:241
  61.1 0.2 copy.32
  61.3 2.3 %convolution_convert_fusion.2 = bf16[128,512]{1,0:T(8,128)(2,1)S(1)} fusion(bf16[2048,512]{1,0:T(8,128)(2,1)} %bitcast.221, bf16[128,2048]{1,0:T(8,128)(2,1)} %param.10, f32[2048]{0:T(1024)} %param.12, f32[128]{0:T(128)S(1)} %get-tuple-element.38), kind=kOutput, calls=%fused_computation.40 | convolution fusion | flops 269549568 | bytes 2761216 | tf_op jit(solution)/shard_map/dot_general | solution.py:241
  63.7 0.2 copy.30
  63.9 0.9 pad_maximum_fusion.refs_0_
  64.7 8.3 %shard_map.114 = bf16[8,128,128]{2,1,0:T(8,128)(2,1)} custom-call(bf16[8,128,128]{2,1,0:T(8,128)(2,1)} %pad_maximum_fusion.refs_0_), custom_call_target="tpu_custom_call" | custom-call | tf_op jit(solution)/shard_map/pallas_call | solution.py:226
  73.1 1.1 copy.33
  74.3 1.3 copy.35
  75.6 0.4 reshape.292
  76.1 1.3 copy.37
  77.4 0.4 reshape.294
  77.8 1.8 %bitcast_reduce_fusion = (f32[4,768]{1,0:T(4,128)S(1)}, f32[1024,768,4]{1,0,2:T(8,128)S(1)}) fusion(bf16[768,4,64]{0,2,1:T(8,128)(2,1)S(1)} %reshape.292, bf16[1024,2,1,64]{0,3,2,1:T(8,128)(2,1)S(1)} %bitcast.215), kind=kOutput, calls=%fused_computation.6 | convolution fusion | flops 408941568 | bytes 13119488 | tf_op jit(solution)/shard_map/tgqd,sgd->gqts/dot_general | solution.py:245
  79.6 6.9 %fusion.14 = (f32[4,768]{1,0:T(4,128)S(1)}, f32[4,768]{1,0:T(4,128)S(1)}, f32[1024,768,4]{1,0,2:T(8,128)}) fusion(f32[4,768]{1,0:T(4,128)S(1)} %get-tuple-element.41, f32[1024,768,4]{1,0,2:T(8,128)S(1)} %get-tuple-element.42, bf16[768,4,64]{0,2,1:T(8,128)(2,1)S(1)} %reshape.294, bf16[1024,2,1,64]{0,3,2,1:T(8,128)(2,1)S(1)} %bitcast.216), kind=kOutput, calls=%fused_computation.16 | convolution fusion | flops 418375680 | bytes 25726976 | tf_op jit(solution)/shard_map/tgqd,sgd->gqts/dot_general | solution.py:245
  86.5 1.4 copy-done.1
  88.0 0.6 reshape.295.refs_0_
  88.6 9.0 %shard_map.115 = f32[4,12,768]{2,1,0:T(8,128)} custom-call(f32[12,768]{1,0:T(8,128)} %reshape.295.refs_0_), custom_call_target="tpu_custom_call" | custom-call | tf_op jit(solution)/shard_map/pallas_call | solution.py:226
  97.7 1.2 copy.38
  99.0 6.3 %fusion.40 = bf16[1024,1,64]{0,2,1:T(8,128)(2,1)S(1)} fusion(bf16[768,4,64]{0,2,1:T(8,128)(2,1)S(1)} %reshape.294, f32[4,768]{1,0:T(4,128)S(1)} %get-tuple-element.35, f32[4,768]{1,0:T(4,128)S(1)} %get-tuple-element.41, f32[1024,768,4]{1,0,2:T(8,128)} %copy-done.1), kind=kOutput, calls=%fused_computation.43 | convolution fusion | flops 415301632 | bytes 13131776 | tf_op jit(solution)/shard_map/gqts,tgqd->sgd/dot_general | solution.py:245
  105.3 0.6 copy-done.2
  105.9 6.8 %fusion.7 = bf16[4,768,1024]{1,2,0:T(8,128)(2,1)S(1)} fusion(f32[1024,768,4]{1,0,2:T(8,128)} %get-tuple-element.43, f32[4,768]{1,0:T(4,128)S(1)} %get-tuple-element.36, f32[4,768]{1,0:T(4,128)S(1)} %get-tuple-element.35, f32[4,768]{1,0:T(4,128)S(1)} %get-tuple-element.41, f32[1024,768,4]{1,0,2:T(8,128)S(1)} %copy-done.2), kind=kLoop, calls=%fused_computation.11 | loop fusion | flops 18874368 | bytes 31494144 | tf_op jit(solution)/shard_map/reshape.11
  112.7 2.0 %fusion.43 = bf16[1024,1,64]{0,2,1:T(8,128)(2,1)S(1)} fusion(bf16[768,4,64]{0,2,1:T(8,128)(2,1)S(1)} %reshape.292, bf16[4,768,1024]{1,2,0:T(8,128)(2,1)S(1)} %fusion.7), kind=kOutput, calls=%fused_computation.44 | convolution fusion | flops 402784256 | bytes 6815744 | tf_op jit(solution)/shard_map/gqts,tgqd->sgd/dot_general | solution.py:245
  114.7 1.2 fusion.31
  115.9 2.3 %fusion.28 = bf16[768,1,4,64]{0,3,2,1:T(8,128)(2,1)S(1)} fusion(f32[4,768]{1,0:T(4,128)S(1)} %get-tuple-element.41, f32[1024,768,4]{1,0,2:T(8,128)S(1)} %copy-done.2, f32[768,4]{0,1:T(4,128)S(1)} %bitcast.246, bf16[1024,2,1,64]{0,3,2,1:T(8,128)(2,1)S(1)} %bitcast.218), kind=kOutput, calls=%fused_computation.32 | convolution fusion | flops 412483584 | bytes 13131776 | tf_op jit(solution)/shard_map/gqts,sgd->tgqd/dot_general | solution.py:245
  118.2 0.5 convert_element_type.97
  118.7 1.1 copy.48.refs_1_
  119.8 0.5 convert_element_type.94
  120.2 1.1 copy.47.refs_0_
  121.5 0.2 copy.46
  121.7 0.9 pad_maximum_fusion.1.refs_2_
  122.6 25.4 %shard_map.116 = (bf16[4,192,256]{2,1,0:T(8,128)(2,1)}, bf16[4,192,256]{2,1,0:T(8,128)(2,1)}, bf16[8,128,128]{2,1,0:T(8,128)(2,1)}, bf16[8,4,24,2048]{3,2,1,0:T(8,128)(2,1)}) custom-call(bf16[4,192,256]{2,1,0:T(8,128)(2,1)} %copy.47.refs_0_, bf16[4,192,256]{2,1,0:T(8,128)(2,1)} %copy.48.refs_1_, bf16[8,128,128]{2,1,0:T(8,128)(2,1)} %pad_maximum_fusion.1.refs_2_, ...), custom_call_target="tpu_custom_call" | custom-call | tf_op jit(solution)/shard_map/pallas_call | solution.py:226
  148.0 1.1 reduce_sum.127
  149.0 1.7 reduce_sum.128
  150.7 1.2 slice_bitcast_fusion
  152.2 2.6 %fusion.69 = f32[128,2048]{1,0:T(8,128)S(1)} fusion(bf16[128,512]{0,1:T(8,128)(2,1)S(1)} %bitcast.235, bf16[2048,512]{1,0:T(8,128)(2,1)} %bitcast.222), kind=kOutput, calls=%fused_computation.90 | convolution fusion | flops 268435456 | bytes 3276800 | tf_op jit(solution)/shard_map/dot_general | solution.py:241
  154.8 2.5 %fusion.49 = (f32[128]{0:T(128)S(1)}, f32[128,2048]{1,0:T(8,128)S(1)}) fusion(bf16[128,2048]{1,0:T(8,128)(2,1)S(1)} %copy-done.3, f32[2048]{0:T(1024)S(1)} %copy-done.8, f32[128,2048]{1,0:T(8,128)S(1)} %fusion.69, bf16[128,512]{0,1:T(8,128)(2,1)S(1)} %bitcast.234, bf16[2048,512]{1,0:T(8,128)(2,1)} %bitcast.220), kind=kOutput, calls=%fused_computation.50 | convolution fusion | flops 269746048 | bytes 4858368 | tf_op jit(solution)/shard_map/dot_general | solution.py:241
  157.3 1.3 fusion.48
  158.7 1.4 convolution_convert_fusion
  160.0 15.2 %shard_map.117 = (bf16[8,24,2048]{2,1,0:T(8,128)(2,1)}, bf16[4,2,96,256]{3,2,1,0:T(8,128)(2,1)}) custom-call(bf16[8,24,2048]{2,1,0:T(8,128)(2,1)} %bitcast.214, bf16[2,96,256]{2,1,0:T(8,128)(2,1)} %bitcast.239), custom_call_target="tpu_custom_call" | custom-call | tf_op jit(solution)/shard_map/pallas_call | solution.py:226
  175.2 1.3 convert_reduce_fusion
  176.5 3.3 %fusion.17 = f32[256,2048]{1,0:T(8,128)} fusion(bf16[4,8,24,256]{3,2,1,0:T(8,128)(2,1)} %bitcast.243, bf16[8,4,24,2048]{3,2,1,0:T(8,128)(2,1)S(1)} %copy-done.4), kind=kOutput, calls=%fused_computation.19 | convolution fusion | flops 805306368 | bytes 5636096 | tf_op jit(solution)/shard_map/stlw,tsld->wd/dot_general | solution.py:373
  180.0 0.8 fusion.55
  (31 shorter events, 1.2 us)
Async XLA Ops:
  0.6 21.3 %copy-start = (bf16[2048,256]{1,0:T(8,128)(2,1)S(1)}, bf16[2048,256]{1,0:T(8,128)(2,1)}, u32[]{:S(2)}) copy-start(bf16[2048,256]{1,0:T(8,128)(2,1)} %param.13) | copy-start | bytes 3145732
  79.6 8.3 %copy-start.1 = (f32[1024,768,4]{1,0,2:T(8,128)}, f32[1024,768,4]{1,0,2:T(8,128)S(1)}, u32[]{:S(2)}) copy-start(f32[1024,768,4]{1,0,2:T(8,128)S(1)} %get-tuple-element.42) | copy-start | bytes 37748740
  97.6 8.3 %copy-start.2 = (f32[1024,768,4]{1,0,2:T(8,128)S(1)}, f32[1024,768,4]{1,0,2:T(8,128)}, u32[]{:S(2)}) copy-start(f32[1024,768,4]{1,0,2:T(8,128)} %copy-done.1) | copy-start | bytes 37748740
  115.9 38.9 %copy-start.3 = (bf16[128,2048]{1,0:T(8,128)(2,1)S(1)}, bf16[128,2048]{1,0:T(8,128)(2,1)}, u32[]{:S(2)}) copy-start(bf16[128,2048]{1,0:T(8,128)(2,1)} %param.10) | copy-start | bytes 1572868
  115.9 38.9 %copy-start.8 = (f32[2048]{0:T(1024)S(1)}, f32[2048]{0:T(1024)}, u32[]{:S(2)}) copy-start(f32[2048]{0:T(1024)} %param.12) | copy-start | bytes 24580
  121.7 58.2 %copy-start.5 = (bf16[24,2048]{1,0:T(8,128)(2,1)S(1)}, bf16[24,2048]{1,0:T(8,128)(2,1)}, u32[]{:S(2)}) copy-start(bf16[24,2048]{1,0:T(8,128)(2,1)} %param.9) | copy-start | bytes 294916
  121.7 58.1 %copy-start.7 = (f32[2048]{0:T(1024)S(1)}, f32[2048]{0:T(1024)}, u32[]{:S(2)}) copy-start(f32[2048]{0:T(1024)} %param.11) | copy-start | bytes 24580
  122.6 57.4 %copy-start.6 = (bf16[24,2048]{1,0:T(8,128)(2,1)S(1)}, bf16[24,2048]{1,0:T(8,128)(2,1)}, u32[]{:S(2)}) copy-start(bf16[24,2048]{1,0:T(8,128)(2,1)} %param.17) | copy-start | bytes 294916
  152.2 24.3 %copy-start.4 = (bf16[8,4,24,2048]{3,2,1,0:T(8,128)(2,1)S(1)}, bf16[8,4,24,2048]{3,2,1,0:T(8,128)(2,1)}, u32[]{:S(2)}) copy-start(bf16[8,4,24,2048]{3,2,1,0:T(8,128)(2,1)} %get-tuple-element.28) | copy-start | bytes 9437188
